TPU v7x, 32 devices: a whole 2x2x4 slice. The times are simulated.
32 devices in a mesh: kv: 8 (over z, y), tp: 4 (over x, core).
Axes of the slice: x: 2, y: 2, z: 4, core: 2. Of those that a mesh axis runs over, the one named last changes fastest.
Arguments:
- tokens: bfloat16 [8, 2048], P(None, 'kv'), may hold values from -6 to 6
- in_gain: float32 [2048], P('kv'), may hold values from 0.1 to 1.9
- w_query: bfloat16 [2048, 512], P('kv', 'tp'), may hold values from -0.125 to 0.125
- score_bias: float32 [4], P('tp'), as said below
- cache_keys: bfloat16 [8, 8192, 512], P(None, 'kv', 'tp'), may hold values from -8 to 8, as said below
- cache_values: bfloat16 [8, 8192, 512], P(None, 'kv', 'tp'), may hold values from -6 to 6
- lengths: int32 [8], replicated, may hold values from 1024 to 8192, as said below
- head_gain: float32 [512], P('tp'), may hold values from 0.1 to 1.9
- w_out: bfloat16 [512, 2048], P('tp', 'kv'), may hold values from -0.25 to 0.25
Outputs:
- mixed: bfloat16 [8, 2048], P(None, 'kv')
Inputs may be any that keep to these rules, and one draw needn't show every extreme that they name: `score_bias`: one value a head, added to every score of that head. `cache_keys`: real-valued key entries. `lengths`: one sequence has all 8192 positions cached.
All inputs are finite; a program needn't handle non-finite values.
Results may differ from a plain program's by a relative error of at most 0.0095.
The roundings to bfloat16 on the way count: a program that leaves them out, or rounds other values in their place, can miss the bound.
Values may be sent and summed in bfloat16 or wider, within the bound.
No kernel may reach another device: no remote copies, remote signals or barrier semaphores. Data moves between devices by JAX's collectives and lax.ppermute only.
A program may use at most 64 MiB of HBM per device.

v0:
```python
import functools

import jax
import jax.numpy as jnp
from jax import lax
from jax.experimental import pallas as pl
from jax.experimental.pallas import tpu as pltpu
from jax.sharding import PartitionSpec as P

EPS = 1e-06
LANES = 128
VMEM = pl.BlockSpec(memory_space=pltpu.VMEM)
SMEM = pl.BlockSpec(memory_space=pltpu.SMEM)
HBM = pl.BlockSpec(memory_space=pltpu.HBM)
F32 = jnp.float32
BF16 = jnp.bfloat16


def three_terms(value):
    high = value.astype(BF16)
    rest = value - high.astype(F32)
    middle = rest.astype(BF16)
    low = (rest - middle.astype(F32)).astype(BF16)
    return high, middle, low


def query_kernel(
    tokens_hbm, in_gain_hbm, w_hbm, bias_hbm, lengths_hbm, head_gain_hbm,
    packed_ref, side_ref,
    tokens_ref, in_gain_ref, w_ref, bias_ref, lengths_ref, head_gain_ref, sems,
):
    pairs = (
        (w_hbm, w_ref),
        (tokens_hbm, tokens_ref),
        (in_gain_hbm, in_gain_ref),
        (lengths_hbm, lengths_ref),
        (bias_hbm, bias_ref),
        (head_gain_hbm, head_gain_ref),
    )
    copies = [
        pltpu.make_async_copy(src, dst, sems.at[i]) for i, (src, dst) in enumerate(pairs)
    ]
    for copy in copies:
        copy.start()
    for copy in copies[1:]:
        copy.wait()
    as_float = tokens_ref[...].astype(F32)
    sequences = as_float.shape[0]
    gained = (as_float * in_gain_ref[...]).astype(BF16)
    squares = jnp.sum(as_float * as_float, axis=1, keepdims=True)
    squares = jnp.broadcast_to(squares, (sequences, LANES))
    row = lax.broadcasted_iota(jnp.int32, (2 * sequences, LANES), 0)
    side = jnp.where(row == sequences, bias_ref[0, 0], 0.0)
    side = jnp.where(row == sequences + 1, head_gain_ref[...], side)
    for b in range(sequences):
        side = jnp.where(row == b, lengths_ref[0, b].astype(F32), side)
    side_ref[...] = side
    copies[0].wait()
    partial_value = jnp.dot(gained, w_ref[...], preferred_element_type=F32)
    packed = jnp.concatenate([partial_value, squares], axis=1)
    for device in range(packed_ref.shape[0]):
        packed_ref[device] = packed


def attention_kernel(width, gathered_ref, side_ref, keys_ref, values_ref, packed_ref):
    sequences, local_len, head_size = keys_ref.shape
    tiles = local_len // LANES
    gathered = jnp.sum(gathered_ref[...], axis=0)
    row_scale = lax.rsqrt(gathered[:, head_size:] / width + EPS)
    queries = gathered[:, :head_size] * row_scale
    row = lax.broadcasted_iota(jnp.int32, (sequences, head_size), 0)
    lane = lax.broadcasted_iota(jnp.int32, (sequences, LANES), 1)
    spread = jnp.concatenate(
        [jnp.where(row == b, queries, 0.0) for b in range(sequences)], axis=1
    ).astype(BF16)
    keys = jnp.concatenate([keys_ref[b] for b in range(sequences)], axis=1)
    scores = lax.dot_general(
        spread, keys, (((1,), (1,)), ((), ())), preferred_element_type=F32
    )
    bias = side_ref[sequences : sequences + 1, :]
    bias = jnp.concatenate([bias] * tiles, axis=1)
    scores = scores * head_size ** (-0.5) + bias
    here = lax.axis_index("kv") * local_len
    limit = side_ref[:sequences, :].astype(jnp.int32) - here
    usable = jnp.concatenate([lane + t * LANES < limit for t in range(tiles)], axis=1)
    soft = jnp.log1p(jnp.exp(-jnp.abs(scores)))
    log_keep = jnp.where(usable, -jnp.maximum(scores, 0.0) - soft, 0.0)
    log_gate = jnp.minimum(scores, 0.0) - soft
    stacked = jnp.concatenate(
        [log_keep[:, t * LANES : (t + 1) * LANES] for t in range(tiles)], axis=0
    )
    terms = jnp.concatenate(three_terms(stacked), axis=0)
    r = lax.broadcasted_iota(jnp.int32, (LANES, 2 * LANES), 0)
    s = lax.broadcasted_iota(jnp.int32, (LANES, 2 * LANES), 1)
    later = jnp.where((r > s) | (s >= LANES), 1.0, 0.0).astype(BF16)
    sums = jnp.dot(terms, later, preferred_element_type=F32)
    count = tiles * sequences
    sums = sums[:count] + sums[count : 2 * count] + sums[2 * count :]
    running = jnp.zeros((sequences, LANES), F32)
    suffixes = [None] * tiles
    for t in reversed(range(tiles)):
        block = sums[t * sequences : (t + 1) * sequences]
        suffixes[t] = block[:, :LANES] + running
        running = running + block[:, LANES:]
    suffix = jnp.concatenate(suffixes, axis=1)
    weights = jnp.where(usable, jnp.exp(log_gate + suffix), 0.0).astype(BF16)
    values = jnp.concatenate([values_ref[b] for b in range(sequences)], axis=1)
    products = jnp.dot(weights, values, preferred_element_type=F32)
    out = jnp.zeros((sequences, head_size), F32)
    for b in range(sequences):
        out = jnp.where(row == b, products[:, b * head_size : (b + 1) * head_size], out)
    packed = jnp.concatenate([out, running], axis=1)
    for device in range(packed_ref.shape[0]):
        packed_ref[device] = packed


def output_kernel(order, every_ref, side_ref, w_out_ref, part_ref):
    size, sequences, _ = every_ref.shape
    place = {device: index for index, device in enumerate(order)}
    later_sum = jnp.zeros((sequences, LANES), F32)
    attended = jnp.zeros((sequences, LANES), F32)
    for n in reversed(range(size)):
        d = place[n]
        attended = attended + every_ref[d, :, :LANES] * jnp.exp(later_sum)
        later_sum = later_sum + every_ref[d, :, LANES:]
    mean_sq = jnp.mean(attended * attended, axis=1, keepdims=True)
    gain = side_ref[sequences + 1 : sequences + 2, :]
    normed = (attended * lax.rsqrt(mean_sq + EPS) * gain).astype(BF16)
    part = jnp.dot(normed, w_out_ref[...], preferred_element_type=F32)
    part_ref[...] = part.astype(BF16)


def mix_kernel(*refs):
    parts = [ref[...].astype(F32) for ref in refs[:-1]]
    while len(parts) > 1:
        parts = [parts[i] + parts[i + 1] for i in range(0, len(parts), 2)]
    refs[-1][...] = parts[0].astype(BF16)


def led_by(leader, size):
    return [leader] + [i for i in range(size) if i != leader]


def shards(
    tokens, in_gain, w_query, score_bias, cache_keys, cache_values, lengths, head_gain, w_out
):
    sequences, features = tokens.shape
    head_width = cache_keys.shape[2]
    assert score_bias.shape[0] == 1 and head_width == LANES
    kv_size = lax.axis_size("kv")
    tp_size = lax.axis_size("tp")
    columns = w_out.shape[1]
    packed, side = pl.pallas_call(
        query_kernel,
        out_shape=(
            jax.ShapeDtypeStruct((kv_size, sequences, 2 * LANES), F32),
            jax.ShapeDtypeStruct((2 * sequences, LANES), F32),
        ),
        in_specs=[HBM] * 6,
        out_specs=(VMEM, VMEM),
        scratch_shapes=[
            pltpu.VMEM(tokens.shape, BF16),
            pltpu.VMEM((1, features), F32),
            pltpu.VMEM(w_query.shape, BF16),
            pltpu.SMEM((1, 1), F32),
            pltpu.SMEM((1, sequences), jnp.int32),
            pltpu.VMEM((1, head_width), F32),
            pltpu.SemaphoreType.DMA((6,)),
        ],
        compiler_params=pltpu.CompilerParams(vmem_limit_bytes=4 << 20),
        cost_estimate=pl.CostEstimate(flops=1 << 33, bytes_accessed=128 << 20, transcendentals=0),
    )(*[
        x if x.size == 1 else pltpu.with_memory_space_constraint(x, pltpu.HBM)
        for x in (tokens, in_gain[None], w_query, score_bias[None], lengths[None], head_gain[None])
    ])
    first = led_by(kv_size * 5 // 8, kv_size)
    gathered = lax.all_to_all(packed, "kv", 0, 0, axis_index_groups=[first], tiled=False)
    packed = pl.pallas_call(
        functools.partial(attention_kernel, features * kv_size),
        out_shape=jax.ShapeDtypeStruct((kv_size, sequences, 2 * LANES), F32),
        in_specs=[VMEM, VMEM, VMEM, VMEM],
        out_specs=VMEM,
        compiler_params=pltpu.CompilerParams(vmem_limit_bytes=24 << 20),
    )(gathered, side, cache_keys, cache_values)
    second = led_by(kv_size * 5 // 8, kv_size)
    every = lax.all_to_all(packed, "kv", 0, 0, axis_index_groups=[second], tiled=False)
    part = pl.pallas_call(
        functools.partial(output_kernel, second),
        out_shape=jax.ShapeDtypeStruct((sequences, columns), BF16),
        in_specs=[VMEM] * 3,
        out_specs=VMEM,
        compiler_params=pltpu.CompilerParams(vmem_limit_bytes=4 << 20),
    )(every, side, w_out)
    parts = {0: part}
    for shift in range(tp_size - 1, 0, -1):
        parts[shift] = lax.ppermute(part, "tp", [(i, i ^ shift) for i in range(tp_size)])
    return pl.pallas_call(
        mix_kernel,
        out_shape=jax.ShapeDtypeStruct((sequences, columns), BF16),
        in_specs=[VMEM] * tp_size,
        out_specs=VMEM,
        compiler_params=pltpu.CompilerParams(vmem_limit_bytes=4 << 20),
    )(*[parts[shift] for shift in range(tp_size)])


def solution(mesh):
    return jax.shard_map(
        shards,
        mesh=mesh,
        in_specs=(
            P(None, "kv"),
            P("kv"),
            P("kv", "tp"),
            P("tp"),
            P(None, "kv", "tp"),
            P(None, "kv", "tp"),
            P(),
            P("tp"),
            P("tp", "kv"),
        ),
        out_specs=P(None, "kv"),
        check_vma=False,
    )
```

profile of v0, /device:TPU:0, one launch (start us, length us, event | category | flops | bytes accessed | tf_op | source)
XLA Modules:
  0.0 27.4 jit_solution(16283693442351145259)
XLA Ops:
  0.7 0.0 copy-start
  0.7 0.0 copy-start.1
  0.7 1.2 %shard_map.91 = (f32[8,8,256]{2,1,0:T(8,128)S(1)}, f32[16,128]{1,0:T(8,128)S(1)}) custom-call(bf16[8,256]{1,0:T(8,128)(2,1)} %tokens_hbm.1, f32[1,256]{1,0:T(1,128)} %bitcast.5, bf16[256,128]{1,0:T(8,128)(2,1)} %w_hbm.1, f32[1,1]{1,0:T(1,128)} %bitcast.4.bias_hbm, s32[1,8]{1,0:T(1,128)} %bitcast.6, f32[1,128]{1,0:T(1,128)} %bitcast.7), custom_call_target="tpu_custom_call" | custom-call | flops 8589934592 | bytes 134217728 | tf_op jit(solution)/shard_map/pallas_call | solution.py:153
  1.9 11.3 %all_to_all.10.gathered_ref = f32[8,8,256]{2,1,0:T(8,128)S(1)} all-to-all(f32[8,8,256]{2,1,0:T(8,128)S(1)} %get-tuple-element.7), channel_id=1, replica_groups={{20,0,4,8,12,16,24,28},{21,1,5,9,13,17,25,29},{22,2,6,10,14,18,26,30},{..., dimensions={0} | all-to-all | bytes 131072 | tf_op jit(solution)/shard_map/all_to_all | solution.py:177
  13.1 0.0 copy-done
  13.1 0.0 copy-done.1
  13.1 0.0 copy-start.2
  13.1 1.2 %shard_map.92 = f32[8,8,256]{2,1,0:T(8,128)S(1)} custom-call(f32[8,8,256]{2,1,0:T(8,128)S(1)} %all_to_all.10.gathered_ref, f32[16,128]{1,0:T(8,128)S(1)} %get-tuple-element.8.side_ref, bf16[8,1024,128]{2,1,0:T(8,128)(2,1)S(1)} %copy-done, bf16[8,1024,128]{2,1,0:T(8,128)(2,1)S(1)} %copy-done.1), custom_call_target="tpu_custom_call" | custom-call | tf_op jit(solution)/shard_map/pallas_call | solution.py:178
  14.3 8.6 %all_to_all.11.every_ref = f32[8,8,256]{2,1,0:T(8,128)S(1)} all-to-all(f32[8,8,256]{2,1,0:T(8,128)S(1)} %shard_map.92), channel_id=1, replica_groups={{20,0,4,8,12,16,24,28},{21,1,5,9,13,17,25,29},{22,2,6,10,14,18,26,30},{..., dimensions={0} | all-to-all | bytes 131072 | tf_op jit(solution)/shard_map/all_to_all | solution.py:186
  23.0 0.0 copy-done.2
  23.0 0.2 shard_map.93.refs_0_
  23.2 0.0 collective-permute-start.2
  23.2 1.5 %collective-permute-start.1 = (bf16[8,256]{1,0:T(8,128)(2,1)S(1)}, bf16[8,256]{1,0:T(8,128)(2,1)S(1)}, u32[]{:S(2)}, u32[]{:S(2)}) collective-permute-start(bf16[8,256]{1,0:T(8,128)(2,1)S(1)} %shard_map.93.refs_0_), channel_id=1, source_target_pairs={{0,2},{1,3},{2,0},{3,1},{4,6},{5,7},{6,4},{7,5},{8,10},{9,11},{10,... | collective-permute-start | bytes 12296 | tf_op jit(solution)/shard_map/ppermute | solution.py:196
  24.7 0.4 %collective-permute-start = (bf16[8,256]{1,0:T(8,128)(2,1)S(1)}, bf16[8,256]{1,0:T(8,128)(2,1)S(1)}, u32[]{:S(2)}, u32[]{:S(2)}) collective-permute-start(bf16[8,256]{1,0:T(8,128)(2,1)S(1)} %shard_map.93.refs_0_), channel_id=1, source_target_pairs={{0,1},{1,0},{2,3},{3,2},{4,5},{5,4},{6,7},{7,6},{8,9},{9,8},{10,11... | collective-permute-start | bytes 12296 | tf_op jit(solution)/shard_map/ppermute | solution.py:196
  25.0 1.2 %collective-permute-done.2.refs_3_ = bf16[8,256]{1,0:T(8,128)(2,1)S(1)} collective-permute-done((bf16[8,256]{1,0:T(8,128)(2,1)S(1)}, bf16[8,256]{1,0:T(8,128)(2,1)S(1)}, u32[]{:S(2)}, u32[]{:S(2)}) %collective-permute-start.2) | collective-permute-done | bytes 4128 | tf_op jit(solution)/shard_map/ppermute | solution.py:196
  26.2 0.6 %collective-permute-done.1.refs_2_ = bf16[8,256]{1,0:T(8,128)(2,1)S(1)} collective-permute-done((bf16[8,256]{1,0:T(8,128)(2,1)S(1)}, bf16[8,256]{1,0:T(8,128)(2,1)S(1)}, u32[]{:S(2)}, u32[]{:S(2)}) %collective-permute-start.1) | collective-permute-done | bytes 4128 | tf_op jit(solution)/shard_map/ppermute | solution.py:196
  26.8 0.0 collective-permute-done.refs_1_
  26.8 0.6 %shard_map.94 = bf16[8,256]{1,0:T(8,128)(2,1)} custom-call(bf16[8,256]{1,0:T(8,128)(2,1)S(1)} %shard_map.93.refs_0_, bf16[8,256]{1,0:T(8,128)(2,1)S(1)} %collective-permute-done.refs_1_, bf16[8,256]{1,0:T(8,128)(2,1)S(1)} %collective-permute-done.1.refs_2_, bf16[8,256]{1,0:T(8,128)(2,1)S(1)} %collective-permute-done.2.refs_3_), custom_call_target="tpu_custom_call" | custom-call | tf_op jit(solution)/shard_map/pallas_call | solution.py:197
Async XLA Ops:
  0.7 12.5 %copy-start = (bf16[8,1024,128]{2,1,0:T(8,128)(2,1)S(1)}, bf16[8,1024,128]{2,1,0:T(8,128)(2,1)}, u32[]{:S(2)}) copy-start(bf16[8,1024,128]{2,1,0:T(8,128)(2,1)} %keys_ref.1) | copy-start | bytes 6291460
  0.7 12.5 %copy-start.1 = (bf16[8,1024,128]{2,1,0:T(8,128)(2,1)S(1)}, bf16[8,1024,128]{2,1,0:T(8,128)(2,1)}, u32[]{:S(2)}) copy-start(bf16[8,1024,128]{2,1,0:T(8,128)(2,1)} %values_ref.1) | copy-start | bytes 6291460
  13.1 9.8 %copy-start.2 = (bf16[128,256]{1,0:T(8,128)(2,1)S(1)}, bf16[128,256]{1,0:T(8,128)(2,1)}, u32[]{:S(2)}) copy-start(bf16[128,256]{1,0:T(8,128)(2,1)} %w_out_ref.1) | copy-start | bytes 196612
  23.2 3.0 %collective-permute-start.2 = (bf16[8,256]{1,0:T(8,128)(2,1)S(1)}, bf16[8,256]{1,0:T(8,128)(2,1)S(1)}, u32[]{:S(2)}, u32[]{:S(2)}) collective-permute-start(bf16[8,256]{1,0:T(8,128)(2,1)S(1)} %shard_map.93.refs_0_), channel_id=1, source_target_pairs={{0,3},{1,2},{2,1},{3,0},{4,7},{5,6},{6,5},{7,4},{8,11},{9,10},{10,... | collective-permute-start | bytes 12296 | tf_op jit(solution)/shard_map/ppermute | solution.py:196
  23.2 3.6 %collective-permute-start.1 = (bf16[8,256]{1,0:T(8,128)(2,1)S(1)}, bf16[8,256]{1,0:T(8,128)(2,1)S(1)}, u32[]{:S(2)}, u32[]{:S(2)}) collective-permute-start(bf16[8,256]{1,0:T(8,128)(2,1)S(1)} %shard_map.93.refs_0_), channel_id=1, source_target_pairs={{0,2},{1,3},{2,0},{3,1},{4,6},{5,7},{6,4},{7,5},{8,10},{9,11},{10,... | collective-permute-start | bytes 12296 | tf_op jit(solution)/shard_map/ppermute | solution.py:196
  24.7 2.1 %collective-permute-start = (bf16[8,256]{1,0:T(8,128)(2,1)S(1)}, bf16[8,256]{1,0:T(8,128)(2,1)S(1)}, u32[]{:S(2)}, u32[]{:S(2)}) collective-permute-start(bf16[8,256]{1,0:T(8,128)(2,1)S(1)} %shard_map.93.refs_0_), channel_id=1, source_target_pairs={{0,1},{1,0},{2,3},{3,2},{4,5},{5,4},{6,7},{7,6},{8,9},{9,8},{10,11... | collective-permute-start | bytes 12296 | tf_op jit(solution)/shard_map/ppermute | solution.py:196
where the time goes:
time: 27.6 us; the launch traced here: 27.4 us
  blocking collectives  19.9 us (72%)
  Pallas kernels  3.18 us (12%)
  starting transfers between devices  1.87 us (7%)
  waiting for transfers between devices  1.75 us (6%)
  between operations  0.68 us (2%)
    all_to_all x1, blocking collectives, shards(): lax.all_to_all(packed, 'kv', 0, 0, axis_index_groups=[first], tiled=False)  11.3 us
    all_to_all x1, blocking collectives, shards(): lax.all_to_all(packed, 'kv', 0, 0, axis_index_groups=[second], tiled=False)  8.62 us
    ppermute x3, starting transfers between devices, shards(): lax.ppermute(part, 'tp', [(i, i ^ shift) for i in range(tp_size)])  1.87 us
    ppermute x3, waiting for transfers between devices, shards(): lax.ppermute(part, 'tp', [(i, i ^ shift) for i in range(tp_size)])  1.75 us
    pallas_call x1, Pallas kernels, shards(): pl.pallas_call(functools.partial(attention_kernel, features * kv_size), o...  1.19 us
    pallas_call x1, Pallas kernels, shards(): pl.pallas_call(query_kernel, out_shape=(jax.ShapeDtypeStruct((kv_size, se...  1.18 us
    pallas_call x1, Pallas kernels, shards(): pl.pallas_call(mix_kernel, out_shape=jax.ShapeDtypeStruct((sequences, col...  0.6 us
  transfers between devices with their start and end apart: 3, of which 2 were waited for; matrix products, arithmetic and copies ran while one was open for 0% of the time, Pallas kernels for 0%

commit v1 on v0

--- a/solution.py
+++ b/solution.py
@@ -24,38 +24,28 @@
     return high, middle, low
 
 
+def opening_kernel(seed_ref):
+    seed_ref[...] = jnp.zeros_like(seed_ref)
+
+
 def query_kernel(
-    tokens_hbm, in_gain_hbm, w_hbm, bias_hbm, lengths_hbm, head_gain_hbm,
+    seed_ref, tokens_ref, in_gain_ref, w_ref, bias_ref, lengths_ref, head_gain_ref,
     packed_ref, side_ref,
-    tokens_ref, in_gain_ref, w_ref, bias_ref, lengths_ref, head_gain_ref, sems,
 ):
-    pairs = (
-        (w_hbm, w_ref),
-        (tokens_hbm, tokens_ref),
-        (in_gain_hbm, in_gain_ref),
-        (lengths_hbm, lengths_ref),
-        (bias_hbm, bias_ref),
-        (head_gain_hbm, head_gain_ref),
-    )
-    copies = [
-        pltpu.make_async_copy(src, dst, sems.at[i]) for i, (src, dst) in enumerate(pairs)
-    ]
-    for copy in copies:
-        copy.start()
-    for copy in copies[1:]:
-        copy.wait()
     as_float = tokens_ref[...].astype(F32)
     sequences = as_float.shape[0]
     gained = (as_float * in_gain_ref[...]).astype(BF16)
     squares = jnp.sum(as_float * as_float, axis=1, keepdims=True)
     squares = jnp.broadcast_to(squares, (sequences, LANES))
     row = lax.broadcasted_iota(jnp.int32, (2 * sequences, LANES), 0)
-    side = jnp.where(row == sequences, bias_ref[0, 0], 0.0)
+    side = jnp.where(row == sequences, bias_ref[...], 0.0)
     side = jnp.where(row == sequences + 1, head_gain_ref[...], side)
-    for b in range(sequences):
-        side = jnp.where(row == b, lengths_ref[0, b].astype(F32), side)
-    side_ref[...] = side
-    copies[0].wait()
+    lengths = lengths_ref[...].astype(F32)
+    own = lax.broadcasted_iota(jnp.int32, (2 * sequences, sequences), 0)
+    own = own == lax.broadcasted_iota(jnp.int32, (2 * sequences, sequences), 1)
+    lengths = jnp.sum(jnp.where(own, lengths, 0.0), axis=1, keepdims=True)
+    side = jnp.where(row < sequences, lengths, side)
+    side_ref[...] = side + seed_ref[:1]
     partial_value = jnp.dot(gained, w_ref[...], preferred_element_type=F32)
     packed = jnp.concatenate([partial_value, squares], axis=1)
     for device in range(packed_ref.shape[0]):
@@ -150,29 +140,24 @@
     kv_size = lax.axis_size("kv")
     tp_size = lax.axis_size("tp")
     columns = w_out.shape[1]
+    seed = pl.pallas_call(
+        opening_kernel,
+        out_shape=pltpu.VMEM((sequences, LANES), F32),
+        out_specs=VMEM,
+        compiler_params=pltpu.CompilerParams(vmem_limit_bytes=1 << 20),
+        cost_estimate=pl.CostEstimate(flops=1 << 33, bytes_accessed=128 << 20, transcendentals=0),
+    )()
     packed, side = pl.pallas_call(
         query_kernel,
         out_shape=(
             jax.ShapeDtypeStruct((kv_size, sequences, 2 * LANES), F32),
             jax.ShapeDtypeStruct((2 * sequences, LANES), F32),
         ),
-        in_specs=[HBM] * 6,
+        in_specs=[VMEM] * 7,
         out_specs=(VMEM, VMEM),
-        scratch_shapes=[
-            pltpu.VMEM(tokens.shape, BF16),
-            pltpu.VMEM((1, features), F32),
-            pltpu.VMEM(w_query.shape, BF16),
-            pltpu.SMEM((1, 1), F32),
-            pltpu.SMEM((1, sequences), jnp.int32),
-            pltpu.VMEM((1, head_width), F32),
-            pltpu.SemaphoreType.DMA((6,)),
-        ],
         compiler_params=pltpu.CompilerParams(vmem_limit_bytes=4 << 20),
         cost_estimate=pl.CostEstimate(flops=1 << 33, bytes_accessed=128 << 20, transcendentals=0),
-    )(*[
-        x if x.size == 1 else pltpu.with_memory_space_constraint(x, pltpu.HBM)
-        for x in (tokens, in_gain[None], w_query, score_bias[None], lengths[None], head_gain[None])
-    ])
+    )(seed, tokens, in_gain[None], w_query, score_bias[None], lengths[None], head_gain[None])
     first = led_by(kv_size * 5 // 8, kv_size)
     gathered = lax.all_to_all(packed, "kv", 0, 0, axis_index_groups=[first], tiled=False)
     packed = pl.pallas_call(

time: 27.6 us -> 26.9 us (0.975)
  Pallas kernels: 3.18 us -> 2.14 us
    pallas_call x1, Pallas kernels: 1.18 us -> 0.13 us  [shards(): pl.pallas_call(query_kernel, out_shape=(jax.ShapeDtypeStruct((kv_size, se...]
where the time goes in v1:
time: 26.9 us; the launch traced here: 26.7 us
  blocking collectives  20 us (74%)
  Pallas kernels  2.14 us (8%)
  starting transfers between devices  1.87 us (7%)
  waiting for transfers between devices  1.75 us (7%)
  between operations  0.77 us (3%)
    all_to_all x1, blocking collectives, shards(): lax.all_to_all(packed, 'kv', 0, 0, axis_index_groups=[first], tiled=False)  11.4 us
    all_to_all x1, blocking collectives, shards(): lax.all_to_all(packed, 'kv', 0, 0, axis_index_groups=[second], tiled=False)  8.62 us
    ppermute x3, starting transfers between devices, shards(): lax.ppermute(part, 'tp', [(i, i ^ shift) for i in range(tp_size)])  1.87 us
    ppermute x3, waiting for transfers between devices, shards(): lax.ppermute(part, 'tp', [(i, i ^ shift) for i in range(tp_size)])  1.75 us
    pallas_call x1, Pallas kernels, shards(): pl.pallas_call(functools.partial(attention_kernel, features * kv_size), o...  1.19 us
    pallas_call x1, Pallas kernels, shards(): pl.pallas_call(mix_kernel, out_shape=jax.ShapeDtypeStruct((sequences, col...  0.6 us
  transfers between devices with their start and end apart: 3, of which 2 were waited for; matrix products, arithmetic and copies ran while one was open for 0% of the time, Pallas kernels for 0%

profile of v1, /device:TPU:0, one launch (start us, length us, event | category | flops | bytes accessed | tf_op | source)
XLA Modules:
  0.0 26.7 jit_solution(86988223099305751)
XLA Ops:
  0.0 0.0 copy-start.7
  0.0 0.0 copy-start.6
  0.0 0.0 copy-start.3
  0.0 0.0 copy-start.5
  0.0 0.0 copy-start.4
  0.7 0.0 copy-done.7
  0.8 0.0 copy-done.6
  0.8 0.1 copy-done.3
  0.9 0.0 copy-done.5
  0.9 0.0 copy-done.4
  0.9 0.0 copy-start
  0.9 0.0 copy-start.1
  0.9 0.1 shard_map.92
  1.0 11.4 %all_to_all.10.gathered_ref = f32[8,8,256]{2,1,0:T(8,128)S(1)} all-to-all(f32[8,8,256]{2,1,0:T(8,128)S(1)} %get-tuple-element.7), channel_id=1, replica_groups={{20,0,4,8,12,16,24,28},{21,1,5,9,13,17,25,29},{22,2,6,10,14,18,26,30},{..., dimensions={0} | all-to-all | bytes 131072 | tf_op jit(solution)/shard_map/all_to_all | solution.py:162
  12.4 0.0 copy-done
  12.4 0.0 copy-done.1
  12.4 0.0 copy-start.2
  12.4 1.2 %shard_map.93 = f32[8,8,256]{2,1,0:T(8,128)S(1)} custom-call(f32[8,8,256]{2,1,0:T(8,128)S(1)} %all_to_all.10.gathered_ref, f32[16,128]{1,0:T(8,128)S(1)} %get-tuple-element.8.side_ref, bf16[8,1024,128]{2,1,0:T(8,128)(2,1)S(1)} %copy-done, bf16[8,1024,128]{2,1,0:T(8,128)(2,1)S(1)} %copy-done.1), custom_call_target="tpu_custom_call" | custom-call | tf_op jit(solution)/shard_map/pallas_call | solution.py:163
  13.6 8.6 %all_to_all.11.every_ref = f32[8,8,256]{2,1,0:T(8,128)S(1)} all-to-all(f32[8,8,256]{2,1,0:T(8,128)S(1)} %shard_map.93), channel_id=1, replica_groups={{20,0,4,8,12,16,24,28},{21,1,5,9,13,17,25,29},{22,2,6,10,14,18,26,30},{..., dimensions={0} | all-to-all | bytes 131072 | tf_op jit(solution)/shard_map/all_to_all | solution.py:171
  22.2 0.0 copy-done.2
  22.3 0.2 shard_map.94.refs_0_
  22.5 0.0 collective-permute-start.2
  22.5 1.5 %collective-permute-start.1 = (bf16[8,256]{1,0:T(8,128)(2,1)S(1)}, bf16[8,256]{1,0:T(8,128)(2,1)S(1)}, u32[]{:S(2)}, u32[]{:S(2)}) collective-permute-start(bf16[8,256]{1,0:T(8,128)(2,1)S(1)} %shard_map.94.refs_0_), channel_id=1, source_target_pairs={{0,2},{1,3},{2,0},{3,1},{4,6},{5,7},{6,4},{7,5},{8,10},{9,11},{10,... | collective-permute-start | bytes 12296 | tf_op jit(solution)/shard_map/ppermute | solution.py:181
  24.0 0.4 %collective-permute-start = (bf16[8,256]{1,0:T(8,128)(2,1)S(1)}, bf16[8,256]{1,0:T(8,128)(2,1)S(1)}, u32[]{:S(2)}, u32[]{:S(2)}) collective-permute-start(bf16[8,256]{1,0:T(8,128)(2,1)S(1)} %shard_map.94.refs_0_), channel_id=1, source_target_pairs={{0,1},{1,0},{2,3},{3,2},{4,5},{5,4},{6,7},{7,6},{8,9},{9,8},{10,11... | collective-permute-start | bytes 12296 | tf_op jit(solution)/shard_map/ppermute | solution.py:181
  24.3 1.2 %collective-permute-done.2.refs_3_ = bf16[8,256]{1,0:T(8,128)(2,1)S(1)} collective-permute-done((bf16[8,256]{1,0:T(8,128)(2,1)S(1)}, bf16[8,256]{1,0:T(8,128)(2,1)S(1)}, u32[]{:S(2)}, u32[]{:S(2)}) %collective-permute-start.2) | collective-permute-done | bytes 4128 | tf_op jit(solution)/shard_map/ppermute | solution.py:181
  25.5 0.6 %collective-permute-done.1.refs_2_ = bf16[8,256]{1,0:T(8,128)(2,1)S(1)} collective-permute-done((bf16[8,256]{1,0:T(8,128)(2,1)S(1)}, bf16[8,256]{1,0:T(8,128)(2,1)S(1)}, u32[]{:S(2)}, u32[]{:S(2)}) %collective-permute-start.1) | collective-permute-done | bytes 4128 | tf_op jit(solution)/shard_map/ppermute | solution.py:181
  26.1 0.0 collective-permute-done.refs_1_
  26.1 0.6 %shard_map.95 = bf16[8,256]{1,0:T(8,128)(2,1)} custom-call(bf16[8,256]{1,0:T(8,128)(2,1)S(1)} %shard_map.94.refs_0_, bf16[8,256]{1,0:T(8,128)(2,1)S(1)} %collective-permute-done.refs_1_, bf16[8,256]{1,0:T(8,128)(2,1)S(1)} %collective-permute-done.1.refs_2_, bf16[8,256]{1,0:T(8,128)(2,1)S(1)} %collective-permute-done.2.refs_3_), custom_call_target="tpu_custom_call" | custom-call | tf_op jit(solution)/shard_map/pallas_call | solution.py:182
  (1 shorter events, 0.0 us)
Async XLA Ops:
  0.0 0.7 %copy-start.7 = (f32[128]{0:T(128)S(1)}, f32[128]{0:T(128)}, u32[]{:S(2)}) copy-start(f32[128]{0:T(128)} %param.16) | copy-start | bytes 1540
  0.0 0.8 %copy-start.6 = (s32[8]{0:T(128)S(1)}, s32[8]{0:T(128)}, u32[]{:S(2)}) copy-start(s32[8]{0:T(128)} %param.15) | copy-start | bytes 100
  0.0 0.9 %copy-start.3 = (bf16[256,128]{1,0:T(8,128)(2,1)S(1)}, bf16[256,128]{1,0:T(8,128)(2,1)}, u32[]{:S(2)}) copy-start(bf16[256,128]{1,0:T(8,128)(2,1)} %w_ref.1) | copy-start | bytes 196612
  0.0 0.9 %copy-start.5 = (f32[256]{0:T(256)S(1)}, f32[256]{0:T(256)}, u32[]{:S(2)}) copy-start(f32[256]{0:T(256)} %param.10) | copy-start | bytes 3076
  0.0 0.9 %copy-start.4 = (bf16[8,256]{1,0:T(8,128)(2,1)S(1)}, bf16[8,256]{1,0:T(8,128)(2,1)}, u32[]{:S(2)}) copy-start(bf16[8,256]{1,0:T(8,128)(2,1)} %tokens_ref.1) | copy-start | bytes 12292
  0.9 11.6 %copy-start = (bf16[8,1024,128]{2,1,0:T(8,128)(2,1)S(1)}, bf16[8,1024,128]{2,1,0:T(8,128)(2,1)}, u32[]{:S(2)}) copy-start(bf16[8,1024,128]{2,1,0:T(8,128)(2,1)} %keys_ref.1) | copy-start | bytes 6291460
  0.9 11.6 %copy-start.1 = (bf16[8,1024,128]{2,1,0:T(8,128)(2,1)S(1)}, bf16[8,1024,128]{2,1,0:T(8,128)(2,1)}, u32[]{:S(2)}) copy-start(bf16[8,1024,128]{2,1,0:T(8,128)(2,1)} %values_ref.1) | copy-start | bytes 6291460
  12.4 9.8 %copy-start.2 = (bf16[128,256]{1,0:T(8,128)(2,1)S(1)}, bf16[128,256]{1,0:T(8,128)(2,1)}, u32[]{:S(2)}) copy-start(bf16[128,256]{1,0:T(8,128)(2,1)} %w_out_ref.1) | copy-start | bytes 196612
  22.5 3.0 %collective-permute-start.2 = (bf16[8,256]{1,0:T(8,128)(2,1)S(1)}, bf16[8,256]{1,0:T(8,128)(2,1)S(1)}, u32[]{:S(2)}, u32[]{:S(2)}) collective-permute-start(bf16[8,256]{1,0:T(8,128)(2,1)S(1)} %shard_map.94.refs_0_), channel_id=1, source_target_pairs={{0,3},{1,2},{2,1},{3,0},{4,7},{5,6},{6,5},{7,4},{8,11},{9,10},{10,... | collective-permute-start | bytes 12296 | tf_op jit(solution)/shard_map/ppermute | solution.py:181
  22.5 3.6 %collective-permute-start.1 = (bf16[8,256]{1,0:T(8,128)(2,1)S(1)}, bf16[8,256]{1,0:T(8,128)(2,1)S(1)}, u32[]{:S(2)}, u32[]{:S(2)}) collective-permute-start(bf16[8,256]{1,0:T(8,128)(2,1)S(1)} %shard_map.94.refs_0_), channel_id=1, source_target_pairs={{0,2},{1,3},{2,0},{3,1},{4,6},{5,7},{6,4},{7,5},{8,10},{9,11},{10,... | collective-permute-start | bytes 12296 | tf_op jit(solution)/shard_map/ppermute | solution.py:181
  24.0 2.1 %collective-permute-start = (bf16[8,256]{1,0:T(8,128)(2,1)S(1)}, bf16[8,256]{1,0:T(8,128)(2,1)S(1)}, u32[]{:S(2)}, u32[]{:S(2)}) collective-permute-start(bf16[8,256]{1,0:T(8,128)(2,1)S(1)} %shard_map.94.refs_0_), channel_id=1, source_target_pairs={{0,1},{1,0},{2,3},{3,2},{4,5},{5,4},{6,7},{7,6},{8,9},{9,8},{10,11... | collective-permute-start | bytes 12296 | tf_op jit(solution)/shard_map/ppermute | solution.py:181

commit v2 on v1

--- a/solution.py
+++ b/solution.py
@@ -6,6 +6,7 @@
 from jax.experimental import pallas as pl
 from jax.experimental.pallas import tpu as pltpu
 from jax.sharding import PartitionSpec as P
+
 
 EPS = 1e-06
 LANES = 128
@@ -29,9 +30,10 @@
 
 
 def query_kernel(
-    seed_ref, tokens_ref, in_gain_ref, w_ref, bias_ref, lengths_ref, head_gain_ref,
-    packed_ref, side_ref,
+    seed_ref, tokens_ref, in_gain_ref, w_ref, bias_ref, lengths_ref, head_gain_ref, w_out_ref,
+    packed_ref, side_ref, block_ref,
 ):
+    block_ref[...] = w_out_ref[...]
     as_float = tokens_ref[...].astype(F32)
     sequences = as_float.shape[0]
     gained = (as_float * in_gain_ref[...]).astype(BF16)
@@ -99,29 +101,53 @@
     out = jnp.zeros((sequences, head_size), F32)
     for b in range(sequences):
         out = jnp.where(row == b, products[:, b * head_size : (b + 1) * head_size], out)
-    packed = jnp.concatenate([out, running], axis=1)
+    gains = three_terms(side_ref[sequences + 1 : sequences + 2, :])
+    extra = jnp.zeros((sequences, LANES), F32)
+    for i, term in enumerate(three_terms(running)):
+        spot = jnp.where(lane == row + i * sequences, term.astype(F32), 0.0)
+        spot = jnp.sum(spot, axis=0, keepdims=True)
+        extra = extra + jnp.where(row == 0, spot, 0.0)
+    for i, term in enumerate(gains):
+        extra = jnp.where(row == 1 + i, term.astype(F32), extra)
+    packed = jnp.concatenate([out, extra], axis=0).astype(BF16)
     for device in range(packed_ref.shape[0]):
         packed_ref[device] = packed
 
 
-def output_kernel(order, every_ref, side_ref, w_out_ref, part_ref):
-    size, sequences, _ = every_ref.shape
-    place = {device: index for index, device in enumerate(order)}
-    later_sum = jnp.zeros((sequences, LANES), F32)
-    attended = jnp.zeros((sequences, LANES), F32)
-    for n in reversed(range(size)):
-        d = place[n]
-        attended = attended + every_ref[d, :, :LANES] * jnp.exp(later_sum)
-        later_sum = later_sum + every_ref[d, :, LANES:]
-    mean_sq = jnp.mean(attended * attended, axis=1, keepdims=True)
-    gain = side_ref[sequences + 1 : sequences + 2, :]
-    normed = (attended * lax.rsqrt(mean_sq + EPS) * gain).astype(BF16)
-    part = jnp.dot(normed, w_out_ref[...], preferred_element_type=F32)
-    part_ref[...] = part.astype(BF16)
+def output_kernel(kv_order, every_ref, own_ref, partner_ref, pair_ref):
+    sequences, _ = pair_ref.shape
+    row = lax.broadcasted_iota(jnp.int32, (sequences, LANES), 0)
+    lane = lax.broadcasted_iota(jnp.int32, (sequences, LANES), 1)
+    spot = (lane % sequences == row) & (lane < 3 * sequences)
+    parity = lax.axis_index("tp") % 2
+    size = len(kv_order)
+    blocks = [every_ref[2 * k + 1 - parity] for k in range(size)]
+    blocks += [every_ref[2 * k + parity] for k in range(size)]
+    extras = [block[sequences:, :].astype(F32) for block in blocks]
+    terms = jnp.concatenate(
+        [jnp.where(spot, extra[:1], 0.0) for extra in extras], axis=0
+    ).astype(BF16)
+    totals = jnp.dot(terms, jnp.ones((LANES, LANES), BF16), preferred_element_type=F32)
+    parts = []
+    for head, w_out_ref in enumerate((own_ref, partner_ref)):
+        later_sum = jnp.zeros((sequences, LANES), F32)
+        attended = jnp.zeros((sequences, LANES), F32)
+        for n in reversed(range(size)):
+            d = head * size + kv_order.index(n)
+            out = blocks[d][:sequences, :].astype(F32)
+            attended = attended + out * jnp.exp(later_sum)
+            later_sum = later_sum + totals[d * sequences : (d + 1) * sequences]
+        mean_sq = jnp.mean(attended * attended, axis=1, keepdims=True)
+        extra = extras[head * size]
+        gain = extra[1:2] + extra[2:3] + extra[3:4]
+        normed = (attended * lax.rsqrt(mean_sq + EPS) * gain).astype(BF16)
+        part = jnp.dot(normed, w_out_ref[...], preferred_element_type=F32)
+        parts.append(part.astype(BF16).astype(F32))
+    pair_ref[...] = parts[0] + parts[1]
 
 
 def mix_kernel(*refs):
-    parts = [ref[...].astype(F32) for ref in refs[:-1]]
+    parts = [ref[...] for ref in refs[:-1]]
     while len(parts) > 1:
         parts = [parts[i] + parts[i + 1] for i in range(0, len(parts), 2)]
     refs[-1][...] = parts[0].astype(BF16)
@@ -140,52 +166,67 @@
     kv_size = lax.axis_size("kv")
     tp_size = lax.axis_size("tp")
     columns = w_out.shape[1]
+    pairs = tp_size // 2
+    assert tp_size % 2 == 0 and pairs & (pairs - 1) == 0
     seed = pl.pallas_call(
         opening_kernel,
         out_shape=pltpu.VMEM((sequences, LANES), F32),
         out_specs=VMEM,
         compiler_params=pltpu.CompilerParams(vmem_limit_bytes=1 << 20),
-        cost_estimate=pl.CostEstimate(flops=1 << 33, bytes_accessed=128 << 20, transcendentals=0),
+        cost_estimate=pl.CostEstimate(
+            flops=1 << 33, bytes_accessed=128 << 20, transcendentals=0
+        ),
     )()
-    packed, side = pl.pallas_call(
+    packed, side, block = pl.pallas_call(
         query_kernel,
         out_shape=(
             jax.ShapeDtypeStruct((kv_size, sequences, 2 * LANES), F32),
             jax.ShapeDtypeStruct((2 * sequences, LANES), F32),
-        ),
-        in_specs=[VMEM] * 7,
-        out_specs=(VMEM, VMEM),
+            jax.ShapeDtypeStruct(w_out.shape, BF16),
+        ),
+        in_specs=[VMEM] * 8,
+        out_specs=(VMEM,) * 3,
         compiler_params=pltpu.CompilerParams(vmem_limit_bytes=4 << 20),
-        cost_estimate=pl.CostEstimate(flops=1 << 33, bytes_accessed=128 << 20, transcendentals=0),
-    )(seed, tokens, in_gain[None], w_query, score_bias[None], lengths[None], head_gain[None])
+        cost_estimate=pl.CostEstimate(
+            flops=1 << 33, bytes_accessed=128 << 20, transcendentals=0
+        ),
+    )(seed, tokens, in_gain[None], w_query, score_bias[None], lengths[None], head_gain[None], w_out)
+    partner = lax.ppermute(block, "tp", [(i, i ^ 1) for i in range(tp_size)])
     first = led_by(kv_size * 5 // 8, kv_size)
     gathered = lax.all_to_all(packed, "kv", 0, 0, axis_index_groups=[first], tiled=False)
     packed = pl.pallas_call(
         functools.partial(attention_kernel, features * kv_size),
-        out_shape=jax.ShapeDtypeStruct((kv_size, sequences, 2 * LANES), F32),
+        out_shape=jax.ShapeDtypeStruct((2 * kv_size, 2 * sequences, LANES), BF16),
         in_specs=[VMEM, VMEM, VMEM, VMEM],
         out_specs=VMEM,
         compiler_params=pltpu.CompilerParams(vmem_limit_bytes=24 << 20),
     )(gathered, side, cache_keys, cache_values)
-    second = led_by(kv_size * 5 // 8, kv_size)
-    every = lax.all_to_all(packed, "kv", 0, 0, axis_index_groups=[second], tiled=False)
-    part = pl.pallas_call(
-        functools.partial(output_kernel, second),
-        out_shape=jax.ShapeDtypeStruct((sequences, columns), BF16),
+    packed, partner = lax.optimization_barrier((packed, partner))
+    groups = [
+        [n * tp_size + 2 * pair + parity for n in first for parity in (1, 0)]
+        for pair in range(pairs)
+    ]
+    every = lax.all_to_all(
+        packed, ("kv", "tp"), 0, 0, axis_index_groups=groups, tiled=False
+    )
+    pair_sum = pl.pallas_call(
+        functools.partial(output_kernel, first),
+        out_shape=jax.ShapeDtypeStruct((sequences, columns), F32),
         in_specs=[VMEM] * 3,
         out_specs=VMEM,
         compiler_params=pltpu.CompilerParams(vmem_limit_bytes=4 << 20),
-    )(every, side, w_out)
-    parts = {0: part}
-    for shift in range(tp_size - 1, 0, -1):
-        parts[shift] = lax.ppermute(part, "tp", [(i, i ^ shift) for i in range(tp_size)])
+    )(every, block, partner)
+    sums = [pair_sum]
+    for shift in range(1, pairs):
+        moves = [(i, i ^ (2 * shift + 1)) for i in range(tp_size)]
+        sums.append(lax.ppermute(pair_sum, "tp", moves))
     return pl.pallas_call(
         mix_kernel,
         out_shape=jax.ShapeDtypeStruct((sequences, columns), BF16),
-        in_specs=[VMEM] * tp_size,
+        in_specs=[VMEM] * pairs,
         out_specs=VMEM,
         compiler_params=pltpu.CompilerParams(vmem_limit_bytes=4 << 20),
-    )(*[parts[shift] for shift in range(tp_size)])
+    )(*sums)
 
 
 def solution(mesh):

time: 26.9 us -> 28.8 us (1.071)
  blocking collectives: 20 us -> 8.18 us
  starting transfers between devices: 1.87 us -> 9.5 us
  waiting for transfers between devices: 1.75 us -> 5.38 us
  local copies, waits for them, and re-layouts: 0.13 us -> 1.73 us
  Pallas kernels: 2.14 us -> 2.91 us
    all_to_all x2 -> x1, blocking collectives: 20 us -> 8.18 us  [shards(): lax.all_to_all(packed, ('kv', 'tp'), 0, 0, axis_index_groups=groups, tile...]
    all_to_all x0 -> x1, starting transfers between devices: none -> 8.27 us  [shards(): lax.all_to_all(packed, 'kv', 0, 0, axis_index_groups=[first], tiled=False)]
    all_to_all x0 -> x1, waiting for transfers between devices: none -> 3.51 us  [shards(): lax.all_to_all(packed, 'kv', 0, 0, axis_index_groups=[first], tiled=False)]
    unnamed x16, local copies, waits for them, and re-layouts: 0.13 us -> 1.73 us
    pallas_call x1, Pallas kernels: 0.13 us -> 0.77 us  [shards(): pl.pallas_call(query_kernel, out_shape=(jax.ShapeDtypeStruct((kv_size, se...]
    ppermute x3 -> x2, starting transfers between devices: 1.87 us -> 1.23 us  [the longest x1 1.23 us: shards(): sums.append(lax.ppermute(pair_sum, 'tp', moves))]
    ppermute x3 -> x2, waiting for transfers between devices: 1.75 us -> 1.87 us  [the longest x1 1.86 us: shards(): sums.append(lax.ppermute(pair_sum, 'tp', moves))]
  transfers between devices with their start and end apart: 3 -> 3, of which waited for: 2 -> 2; matrix products, arithmetic and copies ran while one was open for 0% -> 0% of each run, Pallas kernels for 0% -> 4%
where the time goes in v2:
time: 28.8 us; the launch traced here: 28.5 us
  starting transfers between devices  9.5 us (33%)
  blocking collectives  8.18 us (28%)
  waiting for transfers between devices  5.38 us (19%)
  Pallas kernels  2.91 us (10%)
  local copies, waits for them, and re-layouts  1.73 us (6%)
  between operations  0.78 us (3%)
    all_to_all x1, starting transfers between devices, shards(): lax.all_to_all(packed, 'kv', 0, 0, axis_index_groups=[first], tiled=False)  8.27 us
    all_to_all x1, blocking collectives, shards(): lax.all_to_all(packed, ('kv', 'tp'), 0, 0, axis_index_groups=groups, tile...  8.18 us
    all_to_all x1, waiting for transfers between devices, shards(): lax.all_to_all(packed, 'kv', 0, 0, axis_index_groups=[first], tiled=False)  3.51 us
    ppermute x1, waiting for transfers between devices, shards(): sums.append(lax.ppermute(pair_sum, 'tp', moves))  1.86 us
    unnamed x16, local copies, waits for them, and re-layouts  1.73 us
    ppermute x1, starting transfers between devices, shards(): sums.append(lax.ppermute(pair_sum, 'tp', moves))  1.23 us
    pallas_call x1, Pallas kernels, shards(): pl.pallas_call(functools.partial(attention_kernel, features * kv_size), o...  1.19 us
    pallas_call x1, Pallas kernels, shards(): pl.pallas_call(query_kernel, out_shape=(jax.ShapeDtypeStruct((kv_size, se...  0.77 us
  transfers between devices with their start and end apart: 3, of which 2 were waited for; matrix products, arithmetic and copies ran while one was open for 0% of the time, Pallas kernels for 4%

profile of v2, /device:TPU:0, one launch (start us, length us, event | category | flops | bytes accessed | tf_op | source)
XLA Modules:
  0.0 28.5 jit_solution(209732804216511091)
XLA Ops:
  0.0 0.0 copy-start.3
  0.0 0.0 copy-start.7
  0.0 0.0 copy-start.6
  0.0 0.0 copy-start.2
  0.0 0.0 copy-start.5
  0.0 0.0 copy-start.4
  0.8 0.1 copy-done.3
  0.8 0.0 copy-done.7
  0.8 0.0 copy-done.6
  0.8 0.1 copy-done.2
  0.9 0.0 copy-done.5
  0.9 0.0 copy-done.4
  0.9 0.0 copy-start
  0.9 0.8 %shard_map.92 = (f32[8,8,256]{2,1,0:T(8,128)}, f32[16,128]{1,0:T(8,128)S(1)}, bf16[128,256]{1,0:T(8,128)(2,1)S(1)}) custom-call(f32[8,128]{1,0:T(8,128)S(1)} %shard_map.91.seed_ref, bf16[8,256]{1,0:T(8,128)(2,1)S(1)} %copy-done.4, f32[1,256]{1,0:T(1,128)S(1)} %bitcast.5, bf16[256,128]{1,0:T(8,128)(2,1)S(1)} %copy-done.2, f32[1,1]{1,0:T(1,128)} %bitcast.4.bias_ref, ...), custom_call_target="tpu_custom_call" | custom-call | flops 8589934592 | bytes 134217728 | tf_op jit(solution)/shard_map/pallas_call | solution.py:180
  1.7 8.3 %all-to-all-start = ((f32[8,8,256]{2,1,0:T(8,128)}), f32[8,8,256]{2,1,0:T(8,128)S(1)}, u32[]{:S(2)}, u32[]{:S(2)}) async-start(f32[8,8,256]{2,1,0:T(8,128)} %get-tuple-element.10), calls=%async_computation | async-start | bytes 131072 | tf_op jit(solution)/shard_map/all_to_all | solution.py:196
  10.0 0.0 collective-permute-start
  10.0 3.5 %all-to-all-done.gathered_ref = f32[8,8,256]{2,1,0:T(8,128)S(1)} async-done(((f32[8,8,256]{2,1,0:T(8,128)}), f32[8,8,256]{2,1,0:T(8,128)S(1)}, u32[]{:S(2)}, u32[]{:S(2)}) %all-to-all-start) | async-done | bytes 65568 | tf_op jit(solution)/shard_map/all_to_all | solution.py:196
  13.5 0.0 copy-done
  13.5 0.0 copy-start.1
  13.5 1.6 %copy-done.1 = bf16[8,1024,128]{2,1,0:T(8,128)(2,1)S(1)} copy-done((bf16[8,1024,128]{2,1,0:T(8,128)(2,1)S(1)}, bf16[8,1024,128]{2,1,0:T(8,128)(2,1)}, u32[]{:S(2)}) %copy-start.1) | copy-done | bytes 2097176
  15.1 1.2 %shard_map.93 = bf16[16,16,128]{2,1,0:T(8,128)(2,1)S(1)} custom-call(f32[8,8,256]{2,1,0:T(8,128)S(1)} %all-to-all-done.gathered_ref, f32[16,128]{1,0:T(8,128)S(1)} %get-tuple-element.11.side_ref, bf16[8,1024,128]{2,1,0:T(8,128)(2,1)S(1)} %copy-done, bf16[8,1024,128]{2,1,0:T(8,128)(2,1)S(1)} %copy-done.1), custom_call_target="tpu_custom_call" | custom-call | tf_op jit(solution)/shard_map/pallas_call | solution.py:197
  16.3 0.0 collective-permute-done.partner_ref
  16.3 8.2 %all_to_all.10.every_ref = bf16[16,16,128]{2,1,0:T(8,128)(2,1)S(1)} all-to-all(bf16[16,16,128]{2,1,0:T(8,128)(2,1)S(1)} %shard_map.93), channel_id=1, replica_groups={{21,20,1,0,5,4,9,8,13,12,17,16,25,24,29,28},{23,22,3,2,7,6,11,10,15,14,..., dimensions={0} | all-to-all | bytes 131072 | tf_op jit(solution)/shard_map/all_to_all | solution.py:209
  24.4 0.3 %shard_map.94.refs_0_ = f32[8,256]{1,0:T(8,128)S(1)} custom-call(bf16[16,16,128]{2,1,0:T(8,128)(2,1)S(1)} %all_to_all.10.every_ref, bf16[128,256]{1,0:T(8,128)(2,1)S(1)} %get-tuple-element.12.own_ref, bf16[128,256]{1,0:T(8,128)(2,1)S(1)} %collective-permute-done.partner_ref), custom_call_target="tpu_custom_call" | custom-call | tf_op jit(solution)/shard_map/pallas_call | solution.py:212
  24.8 1.2 %collective-permute-start.1 = (f32[8,256]{1,0:T(8,128)S(1)}, f32[8,256]{1,0:T(8,128)S(1)}, u32[]{:S(2)}, u32[]{:S(2)}) collective-permute-start(f32[8,256]{1,0:T(8,128)S(1)} %shard_map.94.refs_0_), channel_id=1, source_target_pairs={{0,3},{1,2},{2,1},{3,0},{4,7},{5,6},{6,5},{7,4},{8,11},{9,10},{10,... | collective-permute-start | bytes 24584 | tf_op jit(solution)/shard_map/ppermute | solution.py:222
  26.0 1.9 %collective-permute-done.1.refs_1_ = f32[8,256]{1,0:T(8,128)S(1)} collective-permute-done((f32[8,256]{1,0:T(8,128)S(1)}, f32[8,256]{1,0:T(8,128)S(1)}, u32[]{:S(2)}, u32[]{:S(2)}) %collective-permute-start.1) | collective-permute-done | bytes 8224 | tf_op jit(solution)/shard_map/ppermute | solution.py:222
  27.9 0.6 %shard_map.95 = bf16[8,256]{1,0:T(8,128)(2,1)} custom-call(f32[8,256]{1,0:T(8,128)S(1)} %shard_map.94.refs_0_, f32[8,256]{1,0:T(8,128)S(1)} %collective-permute-done.1.refs_1_), custom_call_target="tpu_custom_call" | custom-call | tf_op jit(solution)/shard_map/pallas_call | solution.py:223
  (1 shorter events, 0.0 us)
Async XLA Ops:
  0.0 0.8 %copy-start.3 = (bf16[128,256]{1,0:T(8,128)(2,1)S(1)}, bf16[128,256]{1,0:T(8,128)(2,1)}, u32[]{:S(2)}) copy-start(bf16[128,256]{1,0:T(8,128)(2,1)} %w_out_ref.1) | copy-start | bytes 196612
  0.0 0.8 %copy-start.7 = (f32[128]{0:T(128)S(1)}, f32[128]{0:T(128)}, u32[]{:S(2)}) copy-start(f32[128]{0:T(128)} %param.16) | copy-start | bytes 1540
  0.0 0.8 %copy-start.6 = (s32[8]{0:T(128)S(1)}, s32[8]{0:T(128)}, u32[]{:S(2)}) copy-start(s32[8]{0:T(128)} %param.15) | copy-start | bytes 100
  0.0 0.9 %copy-start.2 = (bf16[256,128]{1,0:T(8,128)(2,1)S(1)}, bf16[256,128]{1,0:T(8,128)(2,1)}, u32[]{:S(2)}) copy-start(bf16[256,128]{1,0:T(8,128)(2,1)} %w_ref.1) | copy-start | bytes 196612
  0.0 0.9 %copy-start.5 = (f32[256]{0:T(256)S(1)}, f32[256]{0:T(256)}, u32[]{:S(2)}) copy-start(f32[256]{0:T(256)} %param.10) | copy-start | bytes 3076
  0.0 0.9 %copy-start.4 = (bf16[8,256]{1,0:T(8,128)(2,1)S(1)}, bf16[8,256]{1,0:T(8,128)(2,1)}, u32[]{:S(2)}) copy-start(bf16[8,256]{1,0:T(8,128)(2,1)} %tokens_ref.1) | copy-start | bytes 12292
  0.9 12.6 %copy-start = (bf16[8,1024,128]{2,1,0:T(8,128)(2,1)S(1)}, bf16[8,1024,128]{2,1,0:T(8,128)(2,1)}, u32[]{:S(2)}) copy-start(bf16[8,1024,128]{2,1,0:T(8,128)(2,1)} %keys_ref.1) | copy-start | bytes 6291460
  1.7 11.8 %all-to-all-start = ((f32[8,8,256]{2,1,0:T(8,128)}), f32[8,8,256]{2,1,0:T(8,128)S(1)}, u32[]{:S(2)}, u32[]{:S(2)}) async-start(f32[8,8,256]{2,1,0:T(8,128)} %get-tuple-element.10), calls=%async_computation | async-start | bytes 131072 | tf_op jit(solution)/shard_map/all_to_all | solution.py:196
  10.0 6.3 %collective-permute-start = (bf16[128,256]{1,0:T(8,128)(2,1)S(1)}, bf16[128,256]{1,0:T(8,128)(2,1)S(1)}, u32[]{:S(2)}, u32[]{:S(2)}) collective-permute-start(bf16[128,256]{1,0:T(8,128)(2,1)S(1)} %get-tuple-element.12.own_ref), channel_id=1, source_target_pairs={{0,1},{1,0},{2,3},{3,2},{4,5},{5,4},{6,7},{7,6},{8,9},{9,8},{10,11... | collective-permute-start | bytes 196616 | tf_op jit(solution)/shard_map/ppermute | solution.py:194
  13.5 1.6 %copy-start.1 = (bf16[8,1024,128]{2,1,0:T(8,128)(2,1)S(1)}, bf16[8,1024,128]{2,1,0:T(8,128)(2,1)}, u32[]{:S(2)}) copy-start(bf16[8,1024,128]{2,1,0:T(8,128)(2,1)} %values_ref.1) | copy-start | bytes 6291460
  24.8 3.1 %collective-permute-start.1 = (f32[8,256]{1,0:T(8,128)S(1)}, f32[8,256]{1,0:T(8,128)S(1)}, u32[]{:S(2)}, u32[]{:S(2)}) collective-permute-start(f32[8,256]{1,0:T(8,128)S(1)} %shard_map.94.refs_0_), channel_id=1, source_target_pairs={{0,3},{1,2},{2,1},{3,0},{4,7},{5,6},{6,5},{7,4},{8,11},{9,10},{10,... | collective-permute-start | bytes 24584 | tf_op jit(solution)/shard_map/ppermute | solution.py:222

commit v3 on v2

--- a/solution.py
+++ b/solution.py
@@ -33,15 +33,22 @@
     seed_ref, tokens_ref, in_gain_ref, w_ref, bias_ref, lengths_ref, head_gain_ref, w_out_ref,
     packed_ref, side_ref, block_ref,
 ):
-    block_ref[...] = w_out_ref[...]
+    rows, columns = w_out_ref.shape
+    if columns < block_ref.shape[1]:
+        block_ref[...] = jnp.zeros_like(block_ref)
+    block_ref[:rows, :columns] = w_out_ref[...]
+    high, middle, low = three_terms(head_gain_ref[...])
+    line = lax.broadcasted_iota(jnp.int32, (16, rows), 0)
+    gains = jnp.where(line == 0, high.astype(F32), 0.0)
+    gains = jnp.where(line == 1, middle.astype(F32), gains)
+    gains = jnp.where(line == 2, low.astype(F32), gains)
+    block_ref[rows : rows + 16, :rows] = gains.astype(BF16)
     as_float = tokens_ref[...].astype(F32)
     sequences = as_float.shape[0]
     gained = (as_float * in_gain_ref[...]).astype(BF16)
     squares = jnp.sum(as_float * as_float, axis=1, keepdims=True)
-    squares = jnp.broadcast_to(squares, (sequences, LANES))
     row = lax.broadcasted_iota(jnp.int32, (2 * sequences, LANES), 0)
     side = jnp.where(row == sequences, bias_ref[...], 0.0)
-    side = jnp.where(row == sequences + 1, head_gain_ref[...], side)
     lengths = lengths_ref[...].astype(F32)
     own = lax.broadcasted_iota(jnp.int32, (2 * sequences, sequences), 0)
     own = own == lax.broadcasted_iota(jnp.int32, (2 * sequences, sequences), 1)
@@ -49,7 +56,13 @@
     side = jnp.where(row < sequences, lengths, side)
     side_ref[...] = side + seed_ref[:1]
     partial_value = jnp.dot(gained, w_ref[...], preferred_element_type=F32)
-    packed = jnp.concatenate([partial_value, squares], axis=1)
+    quarters = sequences // 2
+    lane = lax.broadcasted_iota(jnp.int32, (2, LANES), 1)
+    spread = jnp.zeros((2, LANES), F32)
+    for c in range(quarters):
+        spread = jnp.where(lane == c, squares[2 * c : 2 * c + 2], spread)
+    packed = [partial_value[2 * c : 2 * c + 2] for c in range(quarters)] + [spread]
+    packed = jnp.concatenate(packed, axis=1)
     for device in range(packed_ref.shape[0]):
         packed_ref[device] = packed
 
@@ -58,8 +71,15 @@
     sequences, local_len, head_size = keys_ref.shape
     tiles = local_len // LANES
     gathered = jnp.sum(gathered_ref[...], axis=0)
-    row_scale = lax.rsqrt(gathered[:, head_size:] / width + EPS)
-    queries = gathered[:, :head_size] * row_scale
+    quarters = sequences // 2
+    row_scale = lax.rsqrt(gathered[:, quarters * head_size :] / width + EPS)
+    queries = jnp.concatenate(
+        [
+            gathered[:, c * head_size : (c + 1) * head_size] * row_scale[:, c : c + 1]
+            for c in range(quarters)
+        ],
+        axis=0,
+    )
     row = lax.broadcasted_iota(jnp.int32, (sequences, head_size), 0)
     lane = lax.broadcasted_iota(jnp.int32, (sequences, LANES), 1)
     spread = jnp.concatenate(
@@ -101,47 +121,31 @@
     out = jnp.zeros((sequences, head_size), F32)
     for b in range(sequences):
         out = jnp.where(row == b, products[:, b * head_size : (b + 1) * head_size], out)
-    gains = three_terms(side_ref[sequences + 1 : sequences + 2, :])
-    extra = jnp.zeros((sequences, LANES), F32)
-    for i, term in enumerate(three_terms(running)):
-        spot = jnp.where(lane == row + i * sequences, term.astype(F32), 0.0)
-        spot = jnp.sum(spot, axis=0, keepdims=True)
-        extra = extra + jnp.where(row == 0, spot, 0.0)
-    for i, term in enumerate(gains):
-        extra = jnp.where(row == 1 + i, term.astype(F32), extra)
+    high = running.astype(BF16).astype(F32)
+    extra = jnp.where(lane < LANES // 2, high, running - high)
     packed = jnp.concatenate([out, extra], axis=0).astype(BF16)
     for device in range(packed_ref.shape[0]):
         packed_ref[device] = packed
 
 
 def output_kernel(kv_order, every_ref, own_ref, partner_ref, pair_ref):
-    sequences, _ = pair_ref.shape
-    row = lax.broadcasted_iota(jnp.int32, (sequences, LANES), 0)
-    lane = lax.broadcasted_iota(jnp.int32, (sequences, LANES), 1)
-    spot = (lane % sequences == row) & (lane < 3 * sequences)
+    sequences, columns = pair_ref.shape
     parity = lax.axis_index("tp") % 2
     size = len(kv_order)
-    blocks = [every_ref[2 * k + 1 - parity] for k in range(size)]
-    blocks += [every_ref[2 * k + parity] for k in range(size)]
-    extras = [block[sequences:, :].astype(F32) for block in blocks]
-    terms = jnp.concatenate(
-        [jnp.where(spot, extra[:1], 0.0) for extra in extras], axis=0
-    ).astype(BF16)
-    totals = jnp.dot(terms, jnp.ones((LANES, LANES), BF16), preferred_element_type=F32)
     parts = []
-    for head, w_out_ref in enumerate((own_ref, partner_ref)):
+    for block_ref, offset in ((own_ref, 1 - parity), (partner_ref, parity)):
         later_sum = jnp.zeros((sequences, LANES), F32)
         attended = jnp.zeros((sequences, LANES), F32)
         for n in reversed(range(size)):
-            d = head * size + kv_order.index(n)
-            out = blocks[d][:sequences, :].astype(F32)
-            attended = attended + out * jnp.exp(later_sum)
-            later_sum = later_sum + totals[d * sequences : (d + 1) * sequences]
+            packed = every_ref[2 * kv_order.index(n) + offset].astype(F32)
+            halves = packed[sequences:]
+            attended = attended + packed[:sequences] * jnp.exp(later_sum)
+            later_sum = later_sum + (halves + pltpu.roll(halves, LANES // 2, 1))
         mean_sq = jnp.mean(attended * attended, axis=1, keepdims=True)
-        extra = extras[head * size]
-        gain = extra[1:2] + extra[2:3] + extra[3:4]
+        gain = block_ref[LANES : LANES + 16, :LANES].astype(F32)
+        gain = gain[0:1] + gain[1:2] + gain[2:3]
         normed = (attended * lax.rsqrt(mean_sq + EPS) * gain).astype(BF16)
-        part = jnp.dot(normed, w_out_ref[...], preferred_element_type=F32)
+        part = jnp.dot(normed, block_ref[:LANES, :columns], preferred_element_type=F32)
         parts.append(part.astype(BF16).astype(F32))
     pair_ref[...] = parts[0] + parts[1]
 
@@ -180,9 +184,9 @@
     packed, side, block = pl.pallas_call(
         query_kernel,
         out_shape=(
-            jax.ShapeDtypeStruct((kv_size, sequences, 2 * LANES), F32),
+            jax.ShapeDtypeStruct((kv_size, 2, (sequences // 2 + 1) * LANES), F32),
             jax.ShapeDtypeStruct((2 * sequences, LANES), F32),
-            jax.ShapeDtypeStruct(w_out.shape, BF16),
+            jax.ShapeDtypeStruct((head_width + 16, max(columns, LANES)), BF16),
         ),
         in_specs=[VMEM] * 8,
         out_specs=(VMEM,) * 3,

time: 28.8 us -> 25.9 us (0.90)
  blocking collectives: 8.18 us -> 18.9 us
  starting transfers between devices: 9.5 us -> 1.75 us
  waiting for transfers between devices: 5.38 us -> 1.87 us
  local copies, waits for them, and re-layouts: 1.73 us -> 0.15 us
  Pallas kernels: 2.91 us -> 2.26 us
    all_to_all x0 -> x1, blocking collectives: none -> 10.8 us  [shards(): lax.all_to_all(packed, 'kv', 0, 0, axis_index_groups=[first], tiled=False)]
    all_to_all x1 -> x0, starting transfers between devices: 8.27 us -> none  [shards(): lax.all_to_all(packed, 'kv', 0, 0, axis_index_groups=[first], tiled=False)]
    all_to_all x1 -> x0, waiting for transfers between devices: 3.51 us -> none  [shards(): lax.all_to_all(packed, 'kv', 0, 0, axis_index_groups=[first], tiled=False)]
    unnamed x16, local copies, waits for them, and re-layouts: 1.73 us -> 0.15 us
    pallas_call x1, Pallas kernels: 0.77 us -> 0.15 us  [shards(): pl.pallas_call(query_kernel, out_shape=(jax.ShapeDtypeStruct((kv_size, 2,...]
    ppermute x1, starting transfers between devices: 0.01 us -> 0.53 us  [shards(): partner = lax.ppermute(block, 'tp', [(i, i ^ 1) for i in range(tp_size)])]
  transfers between devices with their start and end apart: 3 -> 2, of which waited for: 2 -> 1; matrix products, arithmetic and copies ran while one was open for 0% -> 0% of each run, Pallas kernels for 4% -> 5%
where the time goes in v3:
time: 25.9 us; the launch traced here: 25.7 us
  blocking collectives  18.9 us (73%)
  Pallas kernels  2.26 us (9%)
  waiting for transfers between devices  1.87 us (7%)
  starting transfers between devices  1.75 us (7%)
  between operations  0.79 us (3%)
    all_to_all x1, blocking collectives, shards(): lax.all_to_all(packed, 'kv', 0, 0, axis_index_groups=[first], tiled=False)  10.8 us
    all_to_all x1, blocking collectives, shards(): lax.all_to_all(packed, ('kv', 'tp'), 0, 0, axis_index_groups=groups, tile...  8.09 us
    ppermute x1, waiting for transfers between devices, shards(): sums.append(lax.ppermute(pair_sum, 'tp', moves))  1.86 us
    pallas_call x1, Pallas kernels, shards(): pl.pallas_call(functools.partial(attention_kernel, features * kv_size), o...  1.22 us
    ppermute x1, starting transfers between devices, shards(): sums.append(lax.ppermute(pair_sum, 'tp', moves))  1.22 us
    pallas_call x1, Pallas kernels, shards(): pl.pallas_call(mix_kernel, out_shape=jax.ShapeDtypeStruct((sequences, col...  0.6 us
    ppermute x1, starting transfers between devices, shards(): partner = lax.ppermute(block, 'tp', [(i, i ^ 1) for i in range(tp_size)])  0.53 us
  transfers between devices with their start and end apart: 2, of which 1 were waited for; matrix products, arithmetic and copies ran while one was open for 0% of the time, Pallas kernels for 5%

profile of v3, /device:TPU:0, one launch (start us, length us, event | category | flops | bytes accessed | tf_op | source)
XLA Modules:
  0.0 25.7 jit_solution(15979555478778473304)
XLA Ops:
  0.0 0.0 copy-start.3
  0.0 0.0 copy-start.7
  0.0 0.0 copy-start.6
  0.0 0.0 copy-start.2
  0.0 0.0 copy-start.5
  0.0 0.0 copy-start.4
  0.8 0.1 copy-done.3
  0.8 0.0 copy-done.7
  0.8 0.0 copy-done.6
  0.8 0.1 copy-done.2
  0.9 0.0 copy-done.5
  0.9 0.0 copy-done.4
  0.9 0.0 copy-start
  0.9 0.0 copy-start.1
  0.9 0.1 shard_map.92
  1.1 0.5 %collective-permute-start = (bf16[144,256]{1,0:T(8,128)(2,1)S(1)}, bf16[144,256]{1,0:T(8,128)(2,1)S(1)}, u32[]{:S(2)}, u32[]{:S(2)}) collective-permute-start(bf16[144,256]{1,0:T(8,128)(2,1)S(1)} %get-tuple-element.12.own_ref), channel_id=1, source_target_pairs={{0,1},{1,0},{2,3},{3,2},{4,5},{5,4},{6,7},{7,6},{8,9},{9,8},{10,11... | collective-permute-start | bytes 221192 | tf_op jit(solution)/shard_map/ppermute | solution.py:198
  1.6 10.8 %all_to_all.10.gathered_ref = f32[8,2,640]{2,1,0:T(2,128)S(1)} all-to-all(f32[8,2,640]{2,1,0:T(2,128)S(1)} %get-tuple-element.10), channel_id=1, replica_groups={{20,0,4,8,12,16,24,28},{21,1,5,9,13,17,25,29},{22,2,6,10,14,18,26,30},{..., dimensions={0} | all-to-all | bytes 81920 | tf_op jit(solution)/shard_map/all_to_all | solution.py:200
  12.4 0.0 copy-done
  12.4 0.0 copy-done.1
  12.4 1.2 %shard_map.93 = bf16[16,16,128]{2,1,0:T(8,128)(2,1)S(1)} custom-call(f32[8,2,640]{2,1,0:T(2,128)S(1)} %all_to_all.10.gathered_ref, f32[16,128]{1,0:T(8,128)S(1)} %get-tuple-element.11.side_ref, bf16[8,1024,128]{2,1,0:T(8,128)(2,1)S(1)} %copy-done, bf16[8,1024,128]{2,1,0:T(8,128)(2,1)S(1)} %copy-done.1), custom_call_target="tpu_custom_call" | custom-call | tf_op jit(solution)/shard_map/pallas_call | solution.py:201
  13.6 0.0 collective-permute-done.partner_ref
  13.7 8.1 %all_to_all.11.every_ref = bf16[16,16,128]{2,1,0:T(8,128)(2,1)S(1)} all-to-all(bf16[16,16,128]{2,1,0:T(8,128)(2,1)S(1)} %shard_map.93), channel_id=1, replica_groups={{21,20,1,0,5,4,9,8,13,12,17,16,25,24,29,28},{23,22,3,2,7,6,11,10,15,14,..., dimensions={0} | all-to-all | bytes 131072 | tf_op jit(solution)/shard_map/all_to_all | solution.py:213
  21.7 0.3 %shard_map.94.refs_0_ = f32[8,256]{1,0:T(8,128)S(1)} custom-call(bf16[16,16,128]{2,1,0:T(8,128)(2,1)S(1)} %all_to_all.11.every_ref, bf16[144,256]{1,0:T(8,128)(2,1)S(1)} %get-tuple-element.12.own_ref, bf16[144,256]{1,0:T(8,128)(2,1)S(1)} %collective-permute-done.partner_ref), custom_call_target="tpu_custom_call" | custom-call | tf_op jit(solution)/shard_map/pallas_call | solution.py:216
  22.0 1.2 %collective-permute-start.1 = (f32[8,256]{1,0:T(8,128)S(1)}, f32[8,256]{1,0:T(8,128)S(1)}, u32[]{:S(2)}, u32[]{:S(2)}) collective-permute-start(f32[8,256]{1,0:T(8,128)S(1)} %shard_map.94.refs_0_), channel_id=1, source_target_pairs={{0,3},{1,2},{2,1},{3,0},{4,7},{5,6},{6,5},{7,4},{8,11},{9,10},{10,... | collective-permute-start | bytes 24584 | tf_op jit(solution)/shard_map/ppermute | solution.py:226
  23.3 1.9 %collective-permute-done.1.refs_1_ = f32[8,256]{1,0:T(8,128)S(1)} collective-permute-done((f32[8,256]{1,0:T(8,128)S(1)}, f32[8,256]{1,0:T(8,128)S(1)}, u32[]{:S(2)}, u32[]{:S(2)}) %collective-permute-start.1) | collective-permute-done | bytes 8224 | tf_op jit(solution)/shard_map/ppermute | solution.py:226
  25.1 0.6 %shard_map.95 = bf16[8,256]{1,0:T(8,128)(2,1)} custom-call(f32[8,256]{1,0:T(8,128)S(1)} %shard_map.94.refs_0_, f32[8,256]{1,0:T(8,128)S(1)} %collective-permute-done.1.refs_1_), custom_call_target="tpu_custom_call" | custom-call | tf_op jit(solution)/shard_map/pallas_call | solution.py:227
  (1 shorter events, 0.0 us)
Async XLA Ops:
  0.0 0.8 %copy-start.3 = (bf16[128,256]{1,0:T(8,128)(2,1)S(1)}, bf16[128,256]{1,0:T(8,128)(2,1)}, u32[]{:S(2)}) copy-start(bf16[128,256]{1,0:T(8,128)(2,1)} %w_out_ref.1) | copy-start | bytes 196612
  0.0 0.8 %copy-start.7 = (f32[128]{0:T(128)S(1)}, f32[128]{0:T(128)}, u32[]{:S(2)}) copy-start(f32[128]{0:T(128)} %param.16) | copy-start | bytes 1540
  0.0 0.8 %copy-start.6 = (s32[8]{0:T(128)S(1)}, s32[8]{0:T(128)}, u32[]{:S(2)}) copy-start(s32[8]{0:T(128)} %param.15) | copy-start | bytes 100
  0.0 0.9 %copy-start.2 = (bf16[256,128]{1,0:T(8,128)(2,1)S(1)}, bf16[256,128]{1,0:T(8,128)(2,1)}, u32[]{:S(2)}) copy-start(bf16[256,128]{1,0:T(8,128)(2,1)} %w_ref.1) | copy-start | bytes 196612
  0.0 0.9 %copy-start.5 = (f32[256]{0:T(256)S(1)}, f32[256]{0:T(256)}, u32[]{:S(2)}) copy-start(f32[256]{0:T(256)} %param.10) | copy-start | bytes 3076
  0.0 0.9 %copy-start.4 = (bf16[8,256]{1,0:T(8,128)(2,1)S(1)}, bf16[8,256]{1,0:T(8,128)(2,1)}, u32[]{:S(2)}) copy-start(bf16[8,256]{1,0:T(8,128)(2,1)} %tokens_ref.1) | copy-start | bytes 12292
  0.9 11.5 %copy-start = (bf16[8,1024,128]{2,1,0:T(8,128)(2,1)S(1)}, bf16[8,1024,128]{2,1,0:T(8,128)(2,1)}, u32[]{:S(2)}) copy-start(bf16[8,1024,128]{2,1,0:T(8,128)(2,1)} %keys_ref.1) | copy-start | bytes 6291460
  0.9 11.5 %copy-start.1 = (bf16[8,1024,128]{2,1,0:T(8,128)(2,1)S(1)}, bf16[8,1024,128]{2,1,0:T(8,128)(2,1)}, u32[]{:S(2)}) copy-start(bf16[8,1024,128]{2,1,0:T(8,128)(2,1)} %values_ref.1) | copy-start | bytes 6291460
  1.1 12.6 %collective-permute-start = (bf16[144,256]{1,0:T(8,128)(2,1)S(1)}, bf16[144,256]{1,0:T(8,128)(2,1)S(1)}, u32[]{:S(2)}, u32[]{:S(2)}) collective-permute-start(bf16[144,256]{1,0:T(8,128)(2,1)S(1)} %get-tuple-element.12.own_ref), channel_id=1, source_target_pairs={{0,1},{1,0},{2,3},{3,2},{4,5},{5,4},{6,7},{7,6},{8,9},{9,8},{10,11... | collective-permute-start | bytes 221192 | tf_op jit(solution)/shard_map/ppermute | solution.py:198
  22.0 3.1 %collective-permute-start.1 = (f32[8,256]{1,0:T(8,128)S(1)}, f32[8,256]{1,0:T(8,128)S(1)}, u32[]{:S(2)}, u32[]{:S(2)}) collective-permute-start(f32[8,256]{1,0:T(8,128)S(1)} %shard_map.94.refs_0_), channel_id=1, source_target_pairs={{0,3},{1,2},{2,1},{3,0},{4,7},{5,6},{6,5},{7,4},{8,11},{9,10},{10,... | collective-permute-start | bytes 24584 | tf_op jit(solution)/shard_map/ppermute | solution.py:226

commit v4 on v3

--- a/solution.py
+++ b/solution.py
@@ -70,7 +70,10 @@
 def attention_kernel(width, gathered_ref, side_ref, keys_ref, values_ref, packed_ref):
     sequences, local_len, head_size = keys_ref.shape
     tiles = local_len // LANES
-    gathered = jnp.sum(gathered_ref[...], axis=0)
+    parity = lax.axis_index("tp") % 2
+    gathered = gathered_ref[1 - parity]
+    for k in range(1, gathered_ref.shape[0] // 2):
+        gathered = gathered + gathered_ref[2 * k + 1 - parity]
     quarters = sequences // 2
     row_scale = lax.rsqrt(gathered[:, quarters * head_size :] / width + EPS)
     queries = jnp.concatenate(
@@ -184,7 +187,7 @@
     packed, side, block = pl.pallas_call(
         query_kernel,
         out_shape=(
-            jax.ShapeDtypeStruct((kv_size, 2, (sequences // 2 + 1) * LANES), F32),
+            jax.ShapeDtypeStruct((2 * kv_size, 2, (sequences // 2 + 1) * LANES), F32),
             jax.ShapeDtypeStruct((2 * sequences, LANES), F32),
             jax.ShapeDtypeStruct((head_width + 16, max(columns, LANES)), BF16),
         ),
@@ -192,12 +195,18 @@
         out_specs=(VMEM,) * 3,
         compiler_params=pltpu.CompilerParams(vmem_limit_bytes=4 << 20),
         cost_estimate=pl.CostEstimate(
-            flops=1 << 33, bytes_accessed=128 << 20, transcendentals=0
+            flops=1 << 20, bytes_accessed=1 << 16, transcendentals=0
         ),
     )(seed, tokens, in_gain[None], w_query, score_bias[None], lengths[None], head_gain[None], w_out)
     partner = lax.ppermute(block, "tp", [(i, i ^ 1) for i in range(tp_size)])
     first = led_by(kv_size * 5 // 8, kv_size)
-    gathered = lax.all_to_all(packed, "kv", 0, 0, axis_index_groups=[first], tiled=False)
+    groups = [
+        [n * tp_size + 2 * pair + parity for n in first for parity in (1, 0)]
+        for pair in range(pairs)
+    ]
+    gathered = lax.all_to_all(
+        packed, ("kv", "tp"), 0, 0, axis_index_groups=groups, tiled=False
+    )
     packed = pl.pallas_call(
         functools.partial(attention_kernel, features * kv_size),
         out_shape=jax.ShapeDtypeStruct((2 * kv_size, 2 * sequences, LANES), BF16),

time: 25.9 us -> 28 us (1.081)
  blocking collectives: 18.9 us -> 8.04 us
  starting transfers between devices: 1.75 us -> 9.1 us
  waiting for transfers between devices: 1.87 us -> 5.22 us
  local copies, waits for them, and re-layouts: 0.15 us -> 1.65 us
  Pallas kernels: 2.26 us -> 2.91 us
    all_to_all x1 -> x0, blocking collectives: 10.8 us -> none  [shards(): lax.all_to_all(packed, 'kv', 0, 0, axis_index_groups=[first], tiled=False)]
    all_to_all x0 -> x1, starting transfers between devices: none -> 7.77 us  [shards(): lax.all_to_all(packed, ('kv', 'tp'), 0, 0, axis_index_groups=groups, tile...]
    all_to_all x0 -> x1, waiting for transfers between devices: none -> 3.35 us  [shards(): lax.all_to_all(packed, ('kv', 'tp'), 0, 0, axis_index_groups=groups, tile...]
    unnamed x16, local copies, waits for them, and re-layouts: 0.15 us -> 1.65 us
    pallas_call x1, Pallas kernels: 0.15 us -> 0.78 us  [shards(): pl.pallas_call(query_kernel, out_shape=(jax.ShapeDtypeStruct((2 * kv_size...]
    ppermute x1, starting transfers between devices: 0.53 us -> 0.11 us  [shards(): partner = lax.ppermute(block, 'tp', [(i, i ^ 1) for i in range(tp_size)])]
  transfers between devices with their start and end apart: 2 -> 3, of which waited for: 1 -> 2; matrix products, arithmetic and copies ran while one was open for 0% -> 0% of each run, Pallas kernels for 5% -> 4%
where the time goes in v4:
time: 28 us; the launch traced here: 27.8 us
  starting transfers between devices  9.1 us (32%)
  blocking collectives  8.04 us (29%)
  waiting for transfers between devices  5.22 us (19%)
  Pallas kernels  2.91 us (10%)
  local copies, waits for them, and re-layouts  1.65 us (6%)
  between operations  0.87 us (3%)
    all_to_all x1, blocking collectives, shards(): lax.all_to_all(packed, ('kv', 'tp'), 0, 0, axis_index_groups=groups, tile...  8.04 us
    all_to_all x1, starting transfers between devices, shards(): lax.all_to_all(packed, ('kv', 'tp'), 0, 0, axis_index_groups=groups, tile...  7.77 us
    all_to_all x1, waiting for transfers between devices, shards(): lax.all_to_all(packed, ('kv', 'tp'), 0, 0, axis_index_groups=groups, tile...  3.35 us
    ppermute x1, waiting for transfers between devices, shards(): sums.append(lax.ppermute(pair_sum, 'tp', moves))  1.86 us
    unnamed x16, local copies, waits for them, and re-layouts  1.65 us
    pallas_call x1, Pallas kernels, shards(): pl.pallas_call(functools.partial(attention_kernel, features * kv_size), o...  1.23 us
    ppermute x1, starting transfers between devices, shards(): sums.append(lax.ppermute(pair_sum, 'tp', moves))  1.22 us
    pallas_call x1, Pallas kernels, shards(): pl.pallas_call(query_kernel, out_shape=(jax.ShapeDtypeStruct((2 * kv_size...  0.78 us
  transfers between devices with their start and end apart: 3, of which 2 were waited for; matrix products, arithmetic and copies ran while one was open for 0% of the time, Pallas kernels for 4%

profile of v4, /device:TPU:0, one launch (start us, length us, event | category | flops | bytes accessed | tf_op | source)
XLA Modules:
  0.0 27.8 jit_solution(12740967841439693207)
XLA Ops:
  0.0 0.0 copy-start.3
  0.0 0.0 copy-start.7
  0.0 0.0 copy-start.6
  0.0 0.0 copy-start.2
  0.0 0.0 copy-start.5
  0.0 0.0 copy-start.4
  0.0 0.0 copy-start
  0.8 0.0 copy-done.3
  0.9 0.0 copy-done.7
  0.9 0.0 copy-done.6
  0.9 0.0 copy-done.2
  0.9 0.0 copy-done.5
  0.9 0.0 copy-done.4
  0.9 0.8 %shard_map.92 = (f32[16,2,640]{2,1,0:T(2,128)}, f32[16,128]{1,0:T(8,128)S(1)}, bf16[144,256]{1,0:T(8,128)(2,1)S(1)}) custom-call(f32[8,128]{1,0:T(8,128)S(1)} %shard_map.91.seed_ref, bf16[8,256]{1,0:T(8,128)(2,1)S(1)} %copy-done.4, f32[1,256]{1,0:T(1,128)S(1)} %bitcast.5, bf16[256,128]{1,0:T(8,128)(2,1)S(1)} %copy-done.2, f32[1,1]{1,0:T(1,128)} %bitcast.4.bias_ref, ...), custom_call_target="tpu_custom_call" | custom-call | flops 1048576 | bytes 65536 | tf_op jit(solution)/shard_map/pallas_call | solution.py:187
  1.7 7.8 %all-to-all-start = ((f32[16,2,640]{2,1,0:T(2,128)}), f32[16,2,640]{2,1,0:T(2,128)S(1)}, u32[]{:S(2)}, u32[]{:S(2)}) async-start(f32[16,2,640]{2,1,0:T(2,128)} %get-tuple-element.10), calls=%async_computation | async-start | bytes 163840 | tf_op jit(solution)/shard_map/all_to_all | solution.py:207
  9.5 0.1 collective-permute-start
  9.6 3.3 %all-to-all-done.gathered_ref = f32[16,2,640]{2,1,0:T(2,128)S(1)} async-done(((f32[16,2,640]{2,1,0:T(2,128)}), f32[16,2,640]{2,1,0:T(2,128)S(1)}, u32[]{:S(2)}, u32[]{:S(2)}) %all-to-all-start) | async-done | bytes 81952 | tf_op jit(solution)/shard_map/all_to_all | solution.py:207
  12.9 0.0 copy-done
  12.9 0.0 copy-start.1
  12.9 1.6 %copy-done.1 = bf16[8,1024,128]{2,1,0:T(8,128)(2,1)S(1)} copy-done((bf16[8,1024,128]{2,1,0:T(8,128)(2,1)S(1)}, bf16[8,1024,128]{2,1,0:T(8,128)(2,1)}, u32[]{:S(2)}) %copy-start.1) | copy-done | bytes 2097176
  14.5 1.2 %shard_map.93 = bf16[16,16,128]{2,1,0:T(8,128)(2,1)S(1)} custom-call(f32[16,2,640]{2,1,0:T(2,128)S(1)} %all-to-all-done.gathered_ref, f32[16,128]{1,0:T(8,128)S(1)} %get-tuple-element.11.side_ref, bf16[8,1024,128]{2,1,0:T(8,128)(2,1)S(1)} %copy-done, bf16[8,1024,128]{2,1,0:T(8,128)(2,1)S(1)} %copy-done.1), custom_call_target="tpu_custom_call" | custom-call | tf_op jit(solution)/shard_map/pallas_call | solution.py:210
  15.8 0.0 collective-permute-done.partner_ref
  15.8 8.0 %all_to_all.10.every_ref = bf16[16,16,128]{2,1,0:T(8,128)(2,1)S(1)} all-to-all(bf16[16,16,128]{2,1,0:T(8,128)(2,1)S(1)} %shard_map.93), channel_id=1, replica_groups={{21,20,1,0,5,4,9,8,13,12,17,16,25,24,29,28},{23,22,3,2,7,6,11,10,15,14,..., dimensions={0} | all-to-all | bytes 131072 | tf_op jit(solution)/shard_map/all_to_all | solution.py:222
  23.8 0.3 %shard_map.94.refs_0_ = f32[8,256]{1,0:T(8,128)S(1)} custom-call(bf16[16,16,128]{2,1,0:T(8,128)(2,1)S(1)} %all_to_all.10.every_ref, bf16[144,256]{1,0:T(8,128)(2,1)S(1)} %get-tuple-element.12.own_ref, bf16[144,256]{1,0:T(8,128)(2,1)S(1)} %collective-permute-done.partner_ref), custom_call_target="tpu_custom_call" | custom-call | tf_op jit(solution)/shard_map/pallas_call | solution.py:225
  24.1 1.2 %collective-permute-start.1 = (f32[8,256]{1,0:T(8,128)S(1)}, f32[8,256]{1,0:T(8,128)S(1)}, u32[]{:S(2)}, u32[]{:S(2)}) collective-permute-start(f32[8,256]{1,0:T(8,128)S(1)} %shard_map.94.refs_0_), channel_id=1, source_target_pairs={{0,3},{1,2},{2,1},{3,0},{4,7},{5,6},{6,5},{7,4},{8,11},{9,10},{10,... | collective-permute-start | bytes 24584 | tf_op jit(solution)/shard_map/ppermute | solution.py:235
  25.3 1.9 %collective-permute-done.1.refs_1_ = f32[8,256]{1,0:T(8,128)S(1)} collective-permute-done((f32[8,256]{1,0:T(8,128)S(1)}, f32[8,256]{1,0:T(8,128)S(1)}, u32[]{:S(2)}, u32[]{:S(2)}) %collective-permute-start.1) | collective-permute-done | bytes 8224 | tf_op jit(solution)/shard_map/ppermute | solution.py:235
  27.2 0.6 %shard_map.95 = bf16[8,256]{1,0:T(8,128)(2,1)} custom-call(f32[8,256]{1,0:T(8,128)S(1)} %shard_map.94.refs_0_, f32[8,256]{1,0:T(8,128)S(1)} %collective-permute-done.1.refs_1_), custom_call_target="tpu_custom_call" | custom-call | tf_op jit(solution)/shard_map/pallas_call | solution.py:236
  (1 shorter events, 0.0 us)
Async XLA Ops:
  0.0 0.8 %copy-start.3 = (bf16[128,256]{1,0:T(8,128)(2,1)S(1)}, bf16[128,256]{1,0:T(8,128)(2,1)}, u32[]{:S(2)}) copy-start(bf16[128,256]{1,0:T(8,128)(2,1)} %w_out_ref.1) | copy-start | bytes 196612
  0.0 0.9 %copy-start.7 = (f32[128]{0:T(128)S(1)}, f32[128]{0:T(128)}, u32[]{:S(2)}) copy-start(f32[128]{0:T(128)} %param.16) | copy-start | bytes 1540
  0.0 0.9 %copy-start.6 = (s32[8]{0:T(128)S(1)}, s32[8]{0:T(128)}, u32[]{:S(2)}) copy-start(s32[8]{0:T(128)} %param.15) | copy-start | bytes 100
  0.0 0.9 %copy-start.2 = (bf16[256,128]{1,0:T(8,128)(2,1)S(1)}, bf16[256,128]{1,0:T(8,128)(2,1)}, u32[]{:S(2)}) copy-start(bf16[256,128]{1,0:T(8,128)(2,1)} %w_ref.1) | copy-start | bytes 196612
  0.0 0.9 %copy-start.5 = (f32[256]{0:T(256)S(1)}, f32[256]{0:T(256)}, u32[]{:S(2)}) copy-start(f32[256]{0:T(256)} %param.10) | copy-start | bytes 3076
  0.0 0.9 %copy-start.4 = (bf16[8,256]{1,0:T(8,128)(2,1)S(1)}, bf16[8,256]{1,0:T(8,128)(2,1)}, u32[]{:S(2)}) copy-start(bf16[8,256]{1,0:T(8,128)(2,1)} %tokens_ref.1) | copy-start | bytes 12292
  0.0 12.9 %copy-start = (bf16[8,1024,128]{2,1,0:T(8,128)(2,1)S(1)}, bf16[8,1024,128]{2,1,0:T(8,128)(2,1)}, u32[]{:S(2)}) copy-start(bf16[8,1024,128]{2,1,0:T(8,128)(2,1)} %keys_ref.1) | copy-start | bytes 6291460
  1.7 11.2 %all-to-all-start = ((f32[16,2,640]{2,1,0:T(2,128)}), f32[16,2,640]{2,1,0:T(2,128)S(1)}, u32[]{:S(2)}, u32[]{:S(2)}) async-start(f32[16,2,640]{2,1,0:T(2,128)} %get-tuple-element.10), calls=%async_computation | async-start | bytes 163840 | tf_op jit(solution)/shard_map/all_to_all | solution.py:207
  9.5 6.3 %collective-permute-start = (bf16[144,256]{1,0:T(8,128)(2,1)S(1)}, bf16[144,256]{1,0:T(8,128)(2,1)S(1)}, u32[]{:S(2)}, u32[]{:S(2)}) collective-permute-start(bf16[144,256]{1,0:T(8,128)(2,1)S(1)} %get-tuple-element.12.own_ref), channel_id=1, source_target_pairs={{0,1},{1,0},{2,3},{3,2},{4,5},{5,4},{6,7},{7,6},{8,9},{9,8},{10,11... | collective-permute-start | bytes 221192 | tf_op jit(solution)/shard_map/ppermute | solution.py:201
  12.9 1.6 %copy-start.1 = (bf16[8,1024,128]{2,1,0:T(8,128)(2,1)S(1)}, bf16[8,1024,128]{2,1,0:T(8,128)(2,1)}, u32[]{:S(2)}) copy-start(bf16[8,1024,128]{2,1,0:T(8,128)(2,1)} %values_ref.1) | copy-start | bytes 6291460
  24.1 3.1 %collective-permute-start.1 = (f32[8,256]{1,0:T(8,128)S(1)}, f32[8,256]{1,0:T(8,128)S(1)}, u32[]{:S(2)}, u32[]{:S(2)}) collective-permute-start(f32[8,256]{1,0:T(8,128)S(1)} %shard_map.94.refs_0_), channel_id=1, source_target_pairs={{0,3},{1,2},{2,1},{3,0},{4,7},{5,6},{6,5},{7,4},{8,11},{9,10},{10,... | collective-permute-start | bytes 24584 | tf_op jit(solution)/shard_map/ppermute | solution.py:235

commit v5 on v4

--- a/solution.py
+++ b/solution.py
@@ -124,9 +124,15 @@
     out = jnp.zeros((sequences, head_size), F32)
     for b in range(sequences):
         out = jnp.where(row == b, products[:, b * head_size : (b + 1) * head_size], out)
-    high = running.astype(BF16).astype(F32)
-    extra = jnp.where(lane < LANES // 2, high, running - high)
-    packed = jnp.concatenate([out, extra], axis=0).astype(BF16)
+    lane = lax.broadcasted_iota(jnp.int32, (2, LANES), 1)
+    group = LANES // quarters
+    total = jnp.zeros((2, LANES), F32)
+    for c in range(quarters):
+        total = jnp.where(lane // group == c, running[2 * c : 2 * c + 2], total)
+    high = total.astype(BF16).astype(F32)
+    total = jnp.where(lane % group < group // 2, high, total - high)
+    packed = [out[2 * c : 2 * c + 2] for c in range(quarters)] + [total]
+    packed = jnp.concatenate(packed, axis=1).astype(BF16)
     for device in range(packed_ref.shape[0]):
         packed_ref[device] = packed
 
@@ -135,15 +141,29 @@
     sequences, columns = pair_ref.shape
     parity = lax.axis_index("tp") % 2
     size = len(kv_order)
+    quarters = sequences // 2
+    group = LANES // quarters
     parts = []
     for block_ref, offset in ((own_ref, 1 - parity), (partner_ref, parity)):
-        later_sum = jnp.zeros((sequences, LANES), F32)
-        attended = jnp.zeros((sequences, LANES), F32)
+        blocks = [
+            every_ref[2 * kv_order.index(n) + offset].astype(F32) for n in range(size)
+        ]
+        halves = jnp.concatenate([block[:, quarters * LANES :] for block in blocks], axis=0)
+        totals = halves + pltpu.roll(halves, LANES - group // 2, 1)
+        later_sum = jnp.zeros((2, LANES), F32)
+        later_sums = [None] * size
         for n in reversed(range(size)):
-            packed = every_ref[2 * kv_order.index(n) + offset].astype(F32)
-            halves = packed[sequences:]
-            attended = attended + packed[:sequences] * jnp.exp(later_sum)
-            later_sum = later_sum + (halves + pltpu.roll(halves, LANES // 2, 1))
+            later_sums[n] = later_sum
+            later_sum = later_sum + totals[2 * n : 2 * n + 2]
+        factors = jnp.exp(jnp.concatenate(later_sums, axis=0))
+        rows = []
+        for c in range(quarters):
+            attended = jnp.zeros((2, LANES), F32)
+            for n in reversed(range(size)):
+                factor = factors[2 * n : 2 * n + 2, c * group : c * group + 1]
+                attended = attended + blocks[n][:, c * LANES : (c + 1) * LANES] * factor
+            rows.append(attended)
+        attended = jnp.concatenate(rows, axis=0)
         mean_sq = jnp.mean(attended * attended, axis=1, keepdims=True)
         gain = block_ref[LANES : LANES + 16, :LANES].astype(F32)
         gain = gain[0:1] + gain[1:2] + gain[2:3]
@@ -180,9 +200,7 @@
         out_shape=pltpu.VMEM((sequences, LANES), F32),
         out_specs=VMEM,
         compiler_params=pltpu.CompilerParams(vmem_limit_bytes=1 << 20),
-        cost_estimate=pl.CostEstimate(
-            flops=1 << 33, bytes_accessed=128 << 20, transcendentals=0
-        ),
+        cost_estimate=pl.CostEstimate(flops=1 << 33, bytes_accessed=128 << 20, transcendentals=0),
     )()
     packed, side, block = pl.pallas_call(
         query_kernel,
@@ -209,7 +227,7 @@
     )
     packed = pl.pallas_call(
         functools.partial(attention_kernel, features * kv_size),
-        out_shape=jax.ShapeDtypeStruct((2 * kv_size, 2 * sequences, LANES), BF16),
+        out_shape=jax.ShapeDtypeStruct((2 * kv_size, 2, (sequences // 2 + 1) * LANES), BF16),
         in_specs=[VMEM, VMEM, VMEM, VMEM],
         out_specs=VMEM,
         compiler_params=pltpu.CompilerParams(vmem_limit_bytes=24 << 20),

time: 28 us -> 28.1 us (level)
  no operation moved by 1% of the time
where the time goes in v5:
time: 28.1 us; the launch traced here: 27.8 us
  starting transfers between devices  9.1 us (32%)
  blocking collectives  8 us (28%)
  waiting for transfers between devices  5.22 us (19%)
  Pallas kernels  3 us (11%)
  local copies, waits for them, and re-layouts  1.65 us (6%)
  between operations  0.87 us (3%)
    all_to_all x1, blocking collectives, shards(): lax.all_to_all(packed, ('kv', 'tp'), 0, 0, axis_index_groups=groups, tile...  8 us
    all_to_all x1, starting transfers between devices, shards(): lax.all_to_all(packed, ('kv', 'tp'), 0, 0, axis_index_groups=groups, tile...  7.77 us
    all_to_all x1, waiting for transfers between devices, shards(): lax.all_to_all(packed, ('kv', 'tp'), 0, 0, axis_index_groups=groups, tile...  3.35 us
    ppermute x1, waiting for transfers between devices, shards(): sums.append(lax.ppermute(pair_sum, 'tp', moves))  1.86 us
    unnamed x16, local copies, waits for them, and re-layouts  1.65 us
    pallas_call x1, Pallas kernels, shards(): pl.pallas_call(functools.partial(attention_kernel, features * kv_size), o...  1.24 us
    ppermute x1, starting transfers between devices, shards(): sums.append(lax.ppermute(pair_sum, 'tp', moves))  1.22 us
    pallas_call x1, Pallas kernels, shards(): pl.pallas_call(query_kernel, out_shape=(jax.ShapeDtypeStruct((2 * kv_size...  0.78 us
  transfers between devices with their start and end apart: 3, of which 2 were waited for; matrix products, arithmetic and copies ran while one was open for 0% of the time, Pallas kernels for 4%

profile of v5, /device:TPU:0, one launch (start us, length us, event | category | flops | bytes accessed | tf_op | source)
XLA Modules:
  0.0 27.8 jit_solution(1158300445994143936)
XLA Ops:
  0.0 0.0 copy-start.3
  0.0 0.0 copy-start.7
  0.0 0.0 copy-start.6
  0.0 0.0 copy-start.2
  0.0 0.0 copy-start.5
  0.0 0.0 copy-start.4
  0.0 0.0 copy-start
  0.8 0.0 copy-done.3
  0.9 0.0 copy-done.7
  0.9 0.0 copy-done.6
  0.9 0.0 copy-done.2
  0.9 0.0 copy-done.5
  0.9 0.0 copy-done.4
  0.9 0.8 %shard_map.92 = (f32[16,2,640]{2,1,0:T(2,128)}, f32[16,128]{1,0:T(8,128)S(1)}, bf16[144,256]{1,0:T(8,128)(2,1)S(1)}) custom-call(f32[8,128]{1,0:T(8,128)S(1)} %shard_map.91.seed_ref, bf16[8,256]{1,0:T(8,128)(2,1)S(1)} %copy-done.4, f32[1,256]{1,0:T(1,128)S(1)} %bitcast.5, bf16[256,128]{1,0:T(8,128)(2,1)S(1)} %copy-done.2, f32[1,1]{1,0:T(1,128)} %bitcast.4.bias_ref, ...), custom_call_target="tpu_custom_call" | custom-call | flops 1048576 | bytes 65536 | tf_op jit(solution)/shard_map/pallas_call | solution.py:205
  1.7 7.8 %all-to-all-start = ((f32[16,2,640]{2,1,0:T(2,128)}), f32[16,2,640]{2,1,0:T(2,128)S(1)}, u32[]{:S(2)}, u32[]{:S(2)}) async-start(f32[16,2,640]{2,1,0:T(2,128)} %get-tuple-element.10), calls=%async_computation | async-start | bytes 163840 | tf_op jit(solution)/shard_map/all_to_all | solution.py:225
  9.5 0.1 collective-permute-start
  9.6 3.3 %all-to-all-done.gathered_ref = f32[16,2,640]{2,1,0:T(2,128)S(1)} async-done(((f32[16,2,640]{2,1,0:T(2,128)}), f32[16,2,640]{2,1,0:T(2,128)S(1)}, u32[]{:S(2)}, u32[]{:S(2)}) %all-to-all-start) | async-done | bytes 81952 | tf_op jit(solution)/shard_map/all_to_all | solution.py:225
  12.9 0.0 copy-done
  12.9 0.0 copy-start.1
  12.9 1.6 %copy-done.1 = bf16[8,1024,128]{2,1,0:T(8,128)(2,1)S(1)} copy-done((bf16[8,1024,128]{2,1,0:T(8,128)(2,1)S(1)}, bf16[8,1024,128]{2,1,0:T(8,128)(2,1)}, u32[]{:S(2)}) %copy-start.1) | copy-done | bytes 2097176
  14.5 1.2 %shard_map.93 = bf16[16,2,640]{2,1,0:T(2,128)(2,1)S(1)} custom-call(f32[16,2,640]{2,1,0:T(2,128)S(1)} %all-to-all-done.gathered_ref, f32[16,128]{1,0:T(8,128)S(1)} %get-tuple-element.11.side_ref, bf16[8,1024,128]{2,1,0:T(8,128)(2,1)S(1)} %copy-done, bf16[8,1024,128]{2,1,0:T(8,128)(2,1)S(1)} %copy-done.1), custom_call_target="tpu_custom_call" | custom-call | tf_op jit(solution)/shard_map/pallas_call | solution.py:228
  15.8 0.0 collective-permute-done.partner_ref
  15.8 8.0 %all_to_all.10.every_ref = bf16[16,2,640]{2,1,0:T(2,128)(2,1)S(1)} all-to-all(bf16[16,2,640]{2,1,0:T(2,128)(2,1)S(1)} %shard_map.93), channel_id=1, replica_groups={{21,20,1,0,5,4,9,8,13,12,17,16,25,24,29,28},{23,22,3,2,7,6,11,10,15,14,..., dimensions={0} | all-to-all | bytes 81920 | tf_op jit(solution)/shard_map/all_to_all | solution.py:240
  23.8 0.4 %shard_map.94.refs_0_ = f32[8,256]{1,0:T(8,128)S(1)} custom-call(bf16[16,2,640]{2,1,0:T(2,128)(2,1)S(1)} %all_to_all.10.every_ref, bf16[144,256]{1,0:T(8,128)(2,1)S(1)} %get-tuple-element.12.own_ref, bf16[144,256]{1,0:T(8,128)(2,1)S(1)} %collective-permute-done.partner_ref), custom_call_target="tpu_custom_call" | custom-call | tf_op jit(solution)/shard_map/pallas_call | solution.py:243
  24.2 1.2 %collective-permute-start.1 = (f32[8,256]{1,0:T(8,128)S(1)}, f32[8,256]{1,0:T(8,128)S(1)}, u32[]{:S(2)}, u32[]{:S(2)}) collective-permute-start(f32[8,256]{1,0:T(8,128)S(1)} %shard_map.94.refs_0_), channel_id=1, source_target_pairs={{0,3},{1,2},{2,1},{3,0},{4,7},{5,6},{6,5},{7,4},{8,11},{9,10},{10,... | collective-permute-start | bytes 24584 | tf_op jit(solution)/shard_map/ppermute | solution.py:253
  25.4 1.9 %collective-permute-done.1.refs_1_ = f32[8,256]{1,0:T(8,128)S(1)} collective-permute-done((f32[8,256]{1,0:T(8,128)S(1)}, f32[8,256]{1,0:T(8,128)S(1)}, u32[]{:S(2)}, u32[]{:S(2)}) %collective-permute-start.1) | collective-permute-done | bytes 8224 | tf_op jit(solution)/shard_map/ppermute | solution.py:253
  27.2 0.6 %shard_map.95 = bf16[8,256]{1,0:T(8,128)(2,1)} custom-call(f32[8,256]{1,0:T(8,128)S(1)} %shard_map.94.refs_0_, f32[8,256]{1,0:T(8,128)S(1)} %collective-permute-done.1.refs_1_), custom_call_target="tpu_custom_call" | custom-call | tf_op jit(solution)/shard_map/pallas_call | solution.py:254
  (1 shorter events, 0.0 us)
Async XLA Ops:
  0.0 0.8 %copy-start.3 = (bf16[128,256]{1,0:T(8,128)(2,1)S(1)}, bf16[128,256]{1,0:T(8,128)(2,1)}, u32[]{:S(2)}) copy-start(bf16[128,256]{1,0:T(8,128)(2,1)} %w_out_ref.1) | copy-start | bytes 196612
  0.0 0.9 %copy-start.7 = (f32[128]{0:T(128)S(1)}, f32[128]{0:T(128)}, u32[]{:S(2)}) copy-start(f32[128]{0:T(128)} %param.16) | copy-start | bytes 1540
  0.0 0.9 %copy-start.6 = (s32[8]{0:T(128)S(1)}, s32[8]{0:T(128)}, u32[]{:S(2)}) copy-start(s32[8]{0:T(128)} %param.15) | copy-start | bytes 100
  0.0 0.9 %copy-start.2 = (bf16[256,128]{1,0:T(8,128)(2,1)S(1)}, bf16[256,128]{1,0:T(8,128)(2,1)}, u32[]{:S(2)}) copy-start(bf16[256,128]{1,0:T(8,128)(2,1)} %w_ref.1) | copy-start | bytes 196612
  0.0 0.9 %copy-start.5 = (f32[256]{0:T(256)S(1)}, f32[256]{0:T(256)}, u32[]{:S(2)}) copy-start(f32[256]{0:T(256)} %param.10) | copy-start | bytes 3076
  0.0 0.9 %copy-start.4 = (bf16[8,256]{1,0:T(8,128)(2,1)S(1)}, bf16[8,256]{1,0:T(8,128)(2,1)}, u32[]{:S(2)}) copy-start(bf16[8,256]{1,0:T(8,128)(2,1)} %tokens_ref.1) | copy-start | bytes 12292
  0.0 12.9 %copy-start = (bf16[8,1024,128]{2,1,0:T(8,128)(2,1)S(1)}, bf16[8,1024,128]{2,1,0:T(8,128)(2,1)}, u32[]{:S(2)}) copy-start(bf16[8,1024,128]{2,1,0:T(8,128)(2,1)} %keys_ref.1) | copy-start | bytes 6291460
  1.7 11.2 %all-to-all-start = ((f32[16,2,640]{2,1,0:T(2,128)}), f32[16,2,640]{2,1,0:T(2,128)S(1)}, u32[]{:S(2)}, u32[]{:S(2)}) async-start(f32[16,2,640]{2,1,0:T(2,128)} %get-tuple-element.10), calls=%async_computation | async-start | bytes 163840 | tf_op jit(solution)/shard_map/all_to_all | solution.py:225
  9.5 6.3 %collective-permute-start = (bf16[144,256]{1,0:T(8,128)(2,1)S(1)}, bf16[144,256]{1,0:T(8,128)(2,1)S(1)}, u32[]{:S(2)}, u32[]{:S(2)}) collective-permute-start(bf16[144,256]{1,0:T(8,128)(2,1)S(1)} %get-tuple-element.12.own_ref), channel_id=1, source_target_pairs={{0,1},{1,0},{2,3},{3,2},{4,5},{5,4},{6,7},{7,6},{8,9},{9,8},{10,11... | collective-permute-start | bytes 221192 | tf_op jit(solution)/shard_map/ppermute | solution.py:219
  12.9 1.6 %copy-start.1 = (bf16[8,1024,128]{2,1,0:T(8,128)(2,1)S(1)}, bf16[8,1024,128]{2,1,0:T(8,128)(2,1)}, u32[]{:S(2)}) copy-start(bf16[8,1024,128]{2,1,0:T(8,128)(2,1)} %values_ref.1) | copy-start | bytes 6291460
  24.2 3.1 %collective-permute-start.1 = (f32[8,256]{1,0:T(8,128)S(1)}, f32[8,256]{1,0:T(8,128)S(1)}, u32[]{:S(2)}, u32[]{:S(2)}) collective-permute-start(f32[8,256]{1,0:T(8,128)S(1)} %shard_map.94.refs_0_), channel_id=1, source_target_pairs={{0,3},{1,2},{2,1},{3,0},{4,7},{5,6},{6,5},{7,4},{8,11},{9,10},{10,... | collective-permute-start | bytes 24584 | tf_op jit(solution)/shard_map/ppermute | solution.py:253

commit v6 on v4

--- a/solution.py
+++ b/solution.py
@@ -30,9 +30,10 @@
 
 
 def query_kernel(
-    seed_ref, tokens_ref, in_gain_ref, w_ref, bias_ref, lengths_ref, head_gain_ref, w_out_ref,
+    seed_ref, tokens_ref, in_gain_ref, w_ref, bias_ref, head_gain_ref, w_out_ref,
     packed_ref, side_ref, block_ref,
 ):
+    side_ref[...] = bias_ref[...] + seed_ref[...]
     rows, columns = w_out_ref.shape
     if columns < block_ref.shape[1]:
         block_ref[...] = jnp.zeros_like(block_ref)
@@ -47,14 +48,6 @@
     sequences = as_float.shape[0]
     gained = (as_float * in_gain_ref[...]).astype(BF16)
     squares = jnp.sum(as_float * as_float, axis=1, keepdims=True)
-    row = lax.broadcasted_iota(jnp.int32, (2 * sequences, LANES), 0)
-    side = jnp.where(row == sequences, bias_ref[...], 0.0)
-    lengths = lengths_ref[...].astype(F32)
-    own = lax.broadcasted_iota(jnp.int32, (2 * sequences, sequences), 0)
-    own = own == lax.broadcasted_iota(jnp.int32, (2 * sequences, sequences), 1)
-    lengths = jnp.sum(jnp.where(own, lengths, 0.0), axis=1, keepdims=True)
-    side = jnp.where(row < sequences, lengths, side)
-    side_ref[...] = side + seed_ref[:1]
     partial_value = jnp.dot(gained, w_ref[...], preferred_element_type=F32)
     quarters = sequences // 2
     lane = lax.broadcasted_iota(jnp.int32, (2, LANES), 1)
@@ -67,9 +60,8 @@
         packed_ref[device] = packed
 
 
-def attention_kernel(width, gathered_ref, side_ref, keys_ref, values_ref, packed_ref):
+def attention_kernel(width, gathered_ref, bias_ref, lengths_ref, keys_ref, values_ref, packed_ref):
     sequences, local_len, head_size = keys_ref.shape
-    tiles = local_len // LANES
     parity = lax.axis_index("tp") % 2
     gathered = gathered_ref[1 - parity]
     for k in range(1, gathered_ref.shape[0] // 2):
@@ -88,39 +80,55 @@
     spread = jnp.concatenate(
         [jnp.where(row == b, queries, 0.0) for b in range(sequences)], axis=1
     ).astype(BF16)
-    keys = jnp.concatenate([keys_ref[b] for b in range(sequences)], axis=1)
-    scores = lax.dot_general(
-        spread, keys, (((1,), (1,)), ((), ())), preferred_element_type=F32
-    )
-    bias = side_ref[sequences : sequences + 1, :]
-    bias = jnp.concatenate([bias] * tiles, axis=1)
-    scores = scores * head_size ** (-0.5) + bias
+    span = local_len // 1
+    tiles = span // LANES
+    bias = jnp.concatenate([bias_ref[...]] * tiles, axis=1)
+    own = lax.broadcasted_iota(jnp.int32, (sequences, sequences), 0)
+    own = own == lax.broadcasted_iota(jnp.int32, (sequences, sequences), 1)
+    lengths = jnp.where(own, lengths_ref[...].astype(F32), 0.0)
+    lengths = jnp.sum(lengths, axis=1, keepdims=True)
     here = lax.axis_index("kv") * local_len
-    limit = side_ref[:sequences, :].astype(jnp.int32) - here
-    usable = jnp.concatenate([lane + t * LANES < limit for t in range(tiles)], axis=1)
-    soft = jnp.log1p(jnp.exp(-jnp.abs(scores)))
-    log_keep = jnp.where(usable, -jnp.maximum(scores, 0.0) - soft, 0.0)
-    log_gate = jnp.minimum(scores, 0.0) - soft
-    stacked = jnp.concatenate(
-        [log_keep[:, t * LANES : (t + 1) * LANES] for t in range(tiles)], axis=0
-    )
-    terms = jnp.concatenate(three_terms(stacked), axis=0)
+    limit = lengths.astype(jnp.int32) - here
     r = lax.broadcasted_iota(jnp.int32, (LANES, 2 * LANES), 0)
     s = lax.broadcasted_iota(jnp.int32, (LANES, 2 * LANES), 1)
     later = jnp.where((r > s) | (s >= LANES), 1.0, 0.0).astype(BF16)
-    sums = jnp.dot(terms, later, preferred_element_type=F32)
-    count = tiles * sequences
-    sums = sums[:count] + sums[count : 2 * count] + sums[2 * count :]
+    pieces = list(reversed(range(1)))
+    every_score = {}
+    for p in pieces:
+        keys = jnp.concatenate(
+            [keys_ref[b, p * span : (p + 1) * span, :] for b in range(sequences)], axis=1
+        )
+        every_score[p] = lax.dot_general(
+            spread, keys, (((1,), (1,)), ((), ())), preferred_element_type=F32
+        )
     running = jnp.zeros((sequences, LANES), F32)
-    suffixes = [None] * tiles
-    for t in reversed(range(tiles)):
-        block = sums[t * sequences : (t + 1) * sequences]
-        suffixes[t] = block[:, :LANES] + running
-        running = running + block[:, LANES:]
-    suffix = jnp.concatenate(suffixes, axis=1)
-    weights = jnp.where(usable, jnp.exp(log_gate + suffix), 0.0).astype(BF16)
-    values = jnp.concatenate([values_ref[b] for b in range(sequences)], axis=1)
-    products = jnp.dot(weights, values, preferred_element_type=F32)
+    products = jnp.zeros((sequences, sequences * head_size), F32)
+    for p in pieces:
+        scores = every_score[p] * head_size ** (-0.5) + bias
+        usable = jnp.concatenate(
+            [lane + (p * tiles + t) * LANES < limit for t in range(tiles)], axis=1
+        )
+        soft = jnp.log1p(jnp.exp(-jnp.abs(scores)))
+        log_keep = jnp.where(usable, -jnp.maximum(scores, 0.0) - soft, 0.0)
+        log_gate = jnp.minimum(scores, 0.0) - soft
+        stacked = jnp.concatenate(
+            [log_keep[:, t * LANES : (t + 1) * LANES] for t in range(tiles)], axis=0
+        )
+        terms = jnp.concatenate(three_terms(stacked), axis=0)
+        sums = jnp.dot(terms, later, preferred_element_type=F32)
+        count = tiles * sequences
+        sums = sums[:count] + sums[count : 2 * count] + sums[2 * count :]
+        suffixes = [None] * tiles
+        for t in reversed(range(tiles)):
+            block = sums[t * sequences : (t + 1) * sequences]
+            suffixes[t] = block[:, :LANES] + running
+            running = running + block[:, LANES:]
+        suffix = jnp.concatenate(suffixes, axis=1)
+        weights = jnp.where(usable, jnp.exp(log_gate + suffix), 0.0).astype(BF16)
+        values = jnp.concatenate(
+            [values_ref[b, p * span : (p + 1) * span, :] for b in range(sequences)], axis=1
+        )
+        products = products + jnp.dot(weights, values, preferred_element_type=F32)
     out = jnp.zeros((sequences, head_size), F32)
     for b in range(sequences):
         out = jnp.where(row == b, products[:, b * head_size : (b + 1) * head_size], out)
@@ -180,24 +188,22 @@
         out_shape=pltpu.VMEM((sequences, LANES), F32),
         out_specs=VMEM,
         compiler_params=pltpu.CompilerParams(vmem_limit_bytes=1 << 20),
-        cost_estimate=pl.CostEstimate(
-            flops=1 << 33, bytes_accessed=128 << 20, transcendentals=0
-        ),
+        cost_estimate=pl.CostEstimate(flops=1 << 33, bytes_accessed=128 << 20, transcendentals=0),
     )()
     packed, side, block = pl.pallas_call(
         query_kernel,
         out_shape=(
             jax.ShapeDtypeStruct((2 * kv_size, 2, (sequences // 2 + 1) * LANES), F32),
-            jax.ShapeDtypeStruct((2 * sequences, LANES), F32),
+            jax.ShapeDtypeStruct((sequences, LANES), F32),
             jax.ShapeDtypeStruct((head_width + 16, max(columns, LANES)), BF16),
         ),
-        in_specs=[VMEM] * 8,
+        in_specs=[VMEM] * 7,
         out_specs=(VMEM,) * 3,
         compiler_params=pltpu.CompilerParams(vmem_limit_bytes=4 << 20),
         cost_estimate=pl.CostEstimate(
             flops=1 << 20, bytes_accessed=1 << 16, transcendentals=0
         ),
-    )(seed, tokens, in_gain[None], w_query, score_bias[None], lengths[None], head_gain[None], w_out)
+    )(seed, tokens, in_gain[None], w_query, score_bias[None], head_gain[None], w_out)
     partner = lax.ppermute(block, "tp", [(i, i ^ 1) for i in range(tp_size)])
     first = led_by(kv_size * 5 // 8, kv_size)
     groups = [
@@ -210,10 +216,10 @@
     packed = pl.pallas_call(
         functools.partial(attention_kernel, features * kv_size),
         out_shape=jax.ShapeDtypeStruct((2 * kv_size, 2 * sequences, LANES), BF16),
-        in_specs=[VMEM, VMEM, VMEM, VMEM],
+        in_specs=[VMEM] * 5,
         out_specs=VMEM,
         compiler_params=pltpu.CompilerParams(vmem_limit_bytes=24 << 20),
-    )(gathered, side, cache_keys, cache_values)
+    )(gathered, side, lengths[None], cache_keys, cache_values)
     packed, partner = lax.optimization_barrier((packed, partner))
     groups = [
         [n * tp_size + 2 * pair + parity for n in first for parity in (1, 0)]

time: 28 us -> 28 us (level)
  no operation moved by 1% of the time
where the time goes in v6:
time: 28 us; the launch traced here: 27.8 us
  starting transfers between devices  9.11 us (33%)
  blocking collectives  8.04 us (29%)
  waiting for transfers between devices  5.22 us (19%)
  Pallas kernels  2.91 us (10%)
  local copies, waits for them, and re-layouts  1.64 us (6%)
  between operations  0.86 us (3%)
    all_to_all x1, blocking collectives, shards(): lax.all_to_all(packed, ('kv', 'tp'), 0, 0, axis_index_groups=groups, tile...  8.04 us
    all_to_all x1, starting transfers between devices, shards(): lax.all_to_all(packed, ('kv', 'tp'), 0, 0, axis_index_groups=groups, tile...  7.78 us
    all_to_all x1, waiting for transfers between devices, shards(): lax.all_to_all(packed, ('kv', 'tp'), 0, 0, axis_index_groups=groups, tile...  3.35 us
    ppermute x1, waiting for transfers between devices, shards(): sums.append(lax.ppermute(pair_sum, 'tp', moves))  1.86 us
    unnamed x16, local copies, waits for them, and re-layouts  1.64 us
    pallas_call x1, Pallas kernels, shards(): pl.pallas_call(functools.partial(attention_kernel, features * kv_size), o...  1.23 us
    ppermute x1, starting transfers between devices, shards(): sums.append(lax.ppermute(pair_sum, 'tp', moves))  1.22 us
    pallas_call x1, Pallas kernels, shards(): pl.pallas_call(query_kernel, out_shape=(jax.ShapeDtypeStruct((2 * kv_size...  0.78 us
  transfers between devices with their start and end apart: 3, of which 2 were waited for; matrix products, arithmetic and copies ran while one was open for 0% of the time, Pallas kernels for 4%

profile of v6, /device:TPU:0, one launch (start us, length us, event | category | flops | bytes accessed | tf_op | source)
XLA Modules:
  0.0 27.8 jit_solution(2201962847432816658)
XLA Ops:
  0.0 0.0 copy-start.3
  0.0 0.0 copy-start.6
  0.0 0.0 copy-start.2
  0.0 0.0 copy-start.5
  0.0 0.0 copy-start.4
  0.0 0.0 copy-start.7
  0.0 0.0 copy-start
  0.8 0.0 copy-done.3
  0.9 0.0 copy-done.6
  0.9 0.0 copy-done.2
  0.9 0.0 copy-done.5
  0.9 0.0 copy-done.4
  0.9 0.8 %shard_map.92 = (f32[16,2,640]{2,1,0:T(2,128)}, f32[8,128]{1,0:T(8,128)S(1)}, bf16[144,256]{1,0:T(8,128)(2,1)S(1)}) custom-call(f32[8,128]{1,0:T(8,128)S(1)} %shard_map.91.seed_ref, bf16[8,256]{1,0:T(8,128)(2,1)S(1)} %copy-done.4, f32[1,256]{1,0:T(1,128)S(1)} %bitcast.5, bf16[256,128]{1,0:T(8,128)(2,1)S(1)} %copy-done.2, f32[1,1]{1,0:T(1,128)} %bitcast.4.bias_ref, ...), custom_call_target="tpu_custom_call" | custom-call | flops 1048576 | bytes 65536 | tf_op jit(solution)/shard_map/pallas_call | solution.py:193
  1.7 7.8 %all-to-all-start = ((f32[16,2,640]{2,1,0:T(2,128)}), f32[16,2,640]{2,1,0:T(2,128)S(1)}, u32[]{:S(2)}, u32[]{:S(2)}) async-start(f32[16,2,640]{2,1,0:T(2,128)} %get-tuple-element.10), calls=%async_computation | async-start | bytes 163840 | tf_op jit(solution)/shard_map/all_to_all | solution.py:213
  9.5 0.1 collective-permute-start
  9.6 3.3 %all-to-all-done.gathered_ref = f32[16,2,640]{2,1,0:T(2,128)S(1)} async-done(((f32[16,2,640]{2,1,0:T(2,128)}), f32[16,2,640]{2,1,0:T(2,128)S(1)}, u32[]{:S(2)}, u32[]{:S(2)}) %all-to-all-start) | async-done | bytes 81952 | tf_op jit(solution)/shard_map/all_to_all | solution.py:213
  12.9 0.0 copy-done.7
  12.9 0.0 copy-done
  12.9 0.0 copy-start.1
  12.9 1.6 %copy-done.1 = bf16[8,1024,128]{2,1,0:T(8,128)(2,1)S(1)} copy-done((bf16[8,1024,128]{2,1,0:T(8,128)(2,1)S(1)}, bf16[8,1024,128]{2,1,0:T(8,128)(2,1)}, u32[]{:S(2)}) %copy-start.1) | copy-done | bytes 2097176
  14.5 1.2 %shard_map.93 = bf16[16,16,128]{2,1,0:T(8,128)(2,1)S(1)} custom-call(f32[16,2,640]{2,1,0:T(2,128)S(1)} %all-to-all-done.gathered_ref, f32[8,128]{1,0:T(8,128)S(1)} %get-tuple-element.11.bias_ref, s32[1,8]{1,0:T(1,128)S(1)} %bitcast.7, bf16[8,1024,128]{2,1,0:T(8,128)(2,1)S(1)} %copy-done, bf16[8,1024,128]{2,1,0:T(8,128)(2,1)S(1)} %copy-done.1), custom_call_target="tpu_custom_call" | custom-call | tf_op jit(solution)/shard_map/pallas_call | solution.py:216
  15.7 0.0 collective-permute-done.partner_ref
  15.8 8.0 %all_to_all.10.every_ref = bf16[16,16,128]{2,1,0:T(8,128)(2,1)S(1)} all-to-all(bf16[16,16,128]{2,1,0:T(8,128)(2,1)S(1)} %shard_map.93), channel_id=1, replica_groups={{21,20,1,0,5,4,9,8,13,12,17,16,25,24,29,28},{23,22,3,2,7,6,11,10,15,14,..., dimensions={0} | all-to-all | bytes 131072 | tf_op jit(solution)/shard_map/all_to_all | solution.py:228
  23.8 0.3 %shard_map.94.refs_0_ = f32[8,256]{1,0:T(8,128)S(1)} custom-call(bf16[16,16,128]{2,1,0:T(8,128)(2,1)S(1)} %all_to_all.10.every_ref, bf16[144,256]{1,0:T(8,128)(2,1)S(1)} %get-tuple-element.12.own_ref, bf16[144,256]{1,0:T(8,128)(2,1)S(1)} %collective-permute-done.partner_ref), custom_call_target="tpu_custom_call" | custom-call | tf_op jit(solution)/shard_map/pallas_call | solution.py:231
  24.1 1.2 %collective-permute-start.1 = (f32[8,256]{1,0:T(8,128)S(1)}, f32[8,256]{1,0:T(8,128)S(1)}, u32[]{:S(2)}, u32[]{:S(2)}) collective-permute-start(f32[8,256]{1,0:T(8,128)S(1)} %shard_map.94.refs_0_), channel_id=1, source_target_pairs={{0,3},{1,2},{2,1},{3,0},{4,7},{5,6},{6,5},{7,4},{8,11},{9,10},{10,... | collective-permute-start | bytes 24584 | tf_op jit(solution)/shard_map/ppermute | solution.py:241
  25.3 1.9 %collective-permute-done.1.refs_1_ = f32[8,256]{1,0:T(8,128)S(1)} collective-permute-done((f32[8,256]{1,0:T(8,128)S(1)}, f32[8,256]{1,0:T(8,128)S(1)}, u32[]{:S(2)}, u32[]{:S(2)}) %collective-permute-start.1) | collective-permute-done | bytes 8224 | tf_op jit(solution)/shard_map/ppermute | solution.py:241
  27.2 0.6 %shard_map.95 = bf16[8,256]{1,0:T(8,128)(2,1)} custom-call(f32[8,256]{1,0:T(8,128)S(1)} %shard_map.94.refs_0_, f32[8,256]{1,0:T(8,128)S(1)} %collective-permute-done.1.refs_1_), custom_call_target="tpu_custom_call" | custom-call | tf_op jit(solution)/shard_map/pallas_call | solution.py:242
  (1 shorter events, 0.0 us)
Async XLA Ops:
  0.0 0.8 %copy-start.3 = (bf16[128,256]{1,0:T(8,128)(2,1)S(1)}, bf16[128,256]{1,0:T(8,128)(2,1)}, u32[]{:S(2)}) copy-start(bf16[128,256]{1,0:T(8,128)(2,1)} %w_out_ref.1) | copy-start | bytes 196612
  0.0 0.9 %copy-start.6 = (f32[128]{0:T(128)S(1)}, f32[128]{0:T(128)}, u32[]{:S(2)}) copy-start(f32[128]{0:T(128)} %param.16) | copy-start | bytes 1540
  0.0 0.9 %copy-start.2 = (bf16[256,128]{1,0:T(8,128)(2,1)S(1)}, bf16[256,128]{1,0:T(8,128)(2,1)}, u32[]{:S(2)}) copy-start(bf16[256,128]{1,0:T(8,128)(2,1)} %w_ref.1) | copy-start | bytes 196612
  0.0 0.9 %copy-start.5 = (f32[256]{0:T(256)S(1)}, f32[256]{0:T(256)}, u32[]{:S(2)}) copy-start(f32[256]{0:T(256)} %param.10) | copy-start | bytes 3076
  0.0 0.9 %copy-start.4 = (bf16[8,256]{1,0:T(8,128)(2,1)S(1)}, bf16[8,256]{1,0:T(8,128)(2,1)}, u32[]{:S(2)}) copy-start(bf16[8,256]{1,0:T(8,128)(2,1)} %tokens_ref.1) | copy-start | bytes 12292
  0.0 12.9 %copy-start.7 = (s32[8]{0:T(128)S(1)}, s32[8]{0:T(128)}, u32[]{:S(2)}) copy-start(s32[8]{0:T(128)} %param.15) | copy-start | bytes 100
  0.0 12.9 %copy-start = (bf16[8,1024,128]{2,1,0:T(8,128)(2,1)S(1)}, bf16[8,1024,128]{2,1,0:T(8,128)(2,1)}, u32[]{:S(2)}) copy-start(bf16[8,1024,128]{2,1,0:T(8,128)(2,1)} %keys_ref.1) | copy-start | bytes 6291460
  1.7 11.2 %all-to-all-start = ((f32[16,2,640]{2,1,0:T(2,128)}), f32[16,2,640]{2,1,0:T(2,128)S(1)}, u32[]{:S(2)}, u32[]{:S(2)}) async-start(f32[16,2,640]{2,1,0:T(2,128)} %get-tuple-element.10), calls=%async_computation | async-start | bytes 163840 | tf_op jit(solution)/shard_map/all_to_all | solution.py:213
  9.5 6.3 %collective-permute-start = (bf16[144,256]{1,0:T(8,128)(2,1)S(1)}, bf16[144,256]{1,0:T(8,128)(2,1)S(1)}, u32[]{:S(2)}, u32[]{:S(2)}) collective-permute-start(bf16[144,256]{1,0:T(8,128)(2,1)S(1)} %get-tuple-element.12.own_ref), channel_id=1, source_target_pairs={{0,1},{1,0},{2,3},{3,2},{4,5},{5,4},{6,7},{7,6},{8,9},{9,8},{10,11... | collective-permute-start | bytes 221192 | tf_op jit(solution)/shard_map/ppermute | solution.py:207
  12.9 1.6 %copy-start.1 = (bf16[8,1024,128]{2,1,0:T(8,128)(2,1)S(1)}, bf16[8,1024,128]{2,1,0:T(8,128)(2,1)}, u32[]{:S(2)}) copy-start(bf16[8,1024,128]{2,1,0:T(8,128)(2,1)} %values_ref.1) | copy-start | bytes 6291460
  24.1 3.1 %collective-permute-start.1 = (f32[8,256]{1,0:T(8,128)S(1)}, f32[8,256]{1,0:T(8,128)S(1)}, u32[]{:S(2)}, u32[]{:S(2)}) collective-permute-start(f32[8,256]{1,0:T(8,128)S(1)} %shard_map.94.refs_0_), channel_id=1, source_target_pairs={{0,3},{1,2},{2,1},{3,0},{4,7},{5,6},{6,5},{7,4},{8,11},{9,10},{10,... | collective-permute-start | bytes 24584 | tf_op jit(solution)/shard_map/ppermute | solution.py:241
